TPU v7x, 256 devices: a whole 4x4x8 slice. The times are simulated.
256 devices in a mesh: gr: 2 (over z_hi), fs: 16 (over z_lo, x), tp: 8 (over y, core).
Axes of the slice: x: 4, y: 4, z: 8 (z_hi: 2, z_lo: 4; z = z_hi * 4 + z_lo), core: 2. Of those that a mesh axis runs over, the one named last changes fastest.
Arguments:
- tokens: bfloat16 [16384, 2048], P(('gr', 'fs')), may hold values from -6 to 6
- routes: int32 [16384, 2], P(('gr', 'fs')), may hold values from 0 to 15, all different within a row; in each aligned block of 512 rows (0 to 511, 512 to 1023, ...) at most 96 rows name the same one
- route_weight: float32 [16384, 2], P(('gr', 'fs')), may hold values from 0.2 to 1
- gain: float32 [2048], P(('gr', 'fs')), may hold values from 0.1 to 1.9
- w_gate: bfloat16 [16, 2048, 4096], P(None, ('gr', 'fs'), 'tp'), may hold values from -0.125 to 0.125
- w_up: bfloat16 [16, 2048, 4096], P(None, ('gr', 'fs'), 'tp'), may hold values from -0.125 to 0.125
- w_down: bfloat16 [16, 2048, 4096], P(None, ('gr', 'fs'), 'tp'), may hold values from -0.09375 to 0.09375
Outputs:
- gate_out: bfloat16 [16, 2048, 4096], P('fs', None, 'tp')
- up_out: bfloat16 [16, 2048, 4096], P('fs', None, 'tp')
- down_out: bfloat16 [16, 2048, 4096], P('fs', None, 'tp')
- mixed: bfloat16 [16384, 2048], P(('gr', 'fs'), 'tp')
Inputs may be any that keep to these rules, and one draw needn't show every extreme that they name: `routes`: each row names two different experts. Among the 512 rows of one device no expert is named more than 96 times, and in every draw some device names some expert exactly 96 times.
All inputs are finite; a program needn't handle non-finite values.
Results may differ from a plain program's by a relative error of at most 0.015.
Values may be sent and summed in bfloat16 or wider, within the bound.
A program may use at most 128 MiB of HBM per device.

v0:
```python
import jax
import jax.numpy as jnp
from jax import lax
from jax.sharding import PartitionSpec as P

D = 2048
EXP_DEV = 1


EPSILON = 1e-05


def sent_together(arrays, axis, split_dim, concat_dim, along):
    widths = [a.shape[along] for a in arrays]
    both = jnp.concatenate(arrays, axis=along)
    whole = lax.all_to_all(both, axis, split_axis=split_dim, concat_axis=concat_dim, tiled=True)
    return tuple(jnp.split(whole, [sum(widths[:k]) for k in range(1, len(widths))], axis=along))


def grouped_exchange(value, axis, split_dim, concat_dim, work, item_dim, out_dim):
    items = jax.tree.leaves(value)[0].shape[item_dim]
    count = 2 if items % 2 == 0 else 1
    outs = []
    for k in range(count):
        group = jax.tree.map(
            lambda a: lax.slice_in_dim(
                a, k * (items // count), (k + 1) * (items // count), axis=item_dim
            ),
            value,
        )
        outs.append(
            work(
                lax.all_to_all(
                    group, axis, split_axis=split_dim, concat_axis=concat_dim, tiled=True
                )
            )
        )
    return jax.tree.map(lambda *parts: jnp.concatenate(parts, axis=out_dim), *outs)


def body(tokens, routes, route_weight, gain, w_gate, w_up, w_down):
    scaling = gain[None, :, None]
    gate_local = (w_gate * scaling).astype(jnp.bfloat16)
    up_local = (w_up * scaling).astype(jnp.bfloat16)
    gate_twice = jnp.concatenate([gate_local, gate_local], axis=0)
    up_twice = jnp.concatenate([up_local, up_local], axis=0)
    down_twice = jnp.concatenate([w_down, w_down], axis=0)
    gate_out, up_out, down_out = sent_together(
        (gate_twice, up_twice, down_twice), ("gr", "fs"), 0, 1, 2
    )
    fs_count = lax.axis_size("fs")
    experts = EXP_DEV * fs_count
    tok_rows = tokens.shape[0]
    capacity = 3 * tok_rows // experts
    float_rows = tokens.astype(jnp.float32)
    normed = (
        float_rows * lax.rsqrt(jnp.mean(float_rows * float_rows, axis=-1, keepdims=True) + EPSILON)
    ).astype(jnp.bfloat16)
    flat_ids = routes.reshape(-1)
    onehot = (flat_ids[:, None] == jnp.arange(experts, dtype=jnp.int32)[None, :]).astype(jnp.int32)
    slot_rank = jnp.sum((jnp.cumsum(onehot, axis=0) - onehot) * onehot, axis=-1)
    destination = (flat_ids * capacity + slot_rank).reshape(tok_rows, 2)
    slot_ids = jnp.arange(experts * capacity, dtype=jnp.int32)
    hits = slot_ids[:, None, None] == destination[None, :, :]
    dispatch = jnp.any(hits, axis=-1).astype(jnp.bfloat16)
    outgoing = jnp.dot(dispatch, normed, preferred_element_type=jnp.float32).astype(jnp.bfloat16)
    outgoing = outgoing.reshape(fs_count, EXP_DEV, capacity, D)

    def expert_work(arrived):
        gate = jnp.einsum("sjnd,jdf->sjnf", arrived, gate_out, preferred_element_type=jnp.float32)
        upper = jnp.einsum("sjnd,jdf->sjnf", arrived, up_out, preferred_element_type=jnp.float32)
        hidden = (jax.nn.silu(gate) * upper).astype(jnp.bfloat16)
        partial_value = jnp.einsum(
            "sjnf,jdf->sjnd", hidden, down_out, preferred_element_type=jnp.float32
        )
        rounded = lax.optimization_barrier(partial_value.astype(jnp.bfloat16))
        summed = lax.psum_scatter(
            rounded.astype(jnp.float32).astype(jnp.bfloat16), "tp", scatter_dimension=3, tiled=True
        )
        return summed

    results = grouped_exchange(outgoing, "fs", 0, 0, expert_work, 2, 2)
    back_home = lax.all_to_all(results, "fs", split_axis=0, concat_axis=0, tiled=True)
    features = back_home.shape[-1]
    flat_back = back_home.reshape(experts * capacity, features).astype(jnp.float32)
    first = jnp.where(slot_ids[None, :] == destination[:, 0:1], route_weight[:, 0:1], 0.0)
    second = jnp.where(slot_ids[None, :] == destination[:, 1:2], route_weight[:, 1:2], 0.0)
    combine_map = first + second
    mixed = jnp.dot(combine_map, flat_back, preferred_element_type=jnp.float32).astype(jnp.bfloat16)
    return (gate_out, up_out, down_out, mixed)


def solution(mesh):
    in_specs = (
        P(("gr", "fs"), None),
        P(("gr", "fs"), None),
        P(("gr", "fs"), None),
        P(("gr", "fs")),
        P(None, ("gr", "fs"), "tp"),
        P(None, ("gr", "fs"), "tp"),
        P(None, ("gr", "fs"), "tp"),
    )
    out_specs = (
        P("fs", None, "tp"),
        P("fs", None, "tp"),
        P("fs", None, "tp"),
        P(("gr", "fs"), "tp"),
    )
    return jax.shard_map(body, mesh=mesh, in_specs=in_specs, out_specs=out_specs, check_vma=False)
```

profile of v0, /device:TPU:1, one launch (start us, length us, event | category | flops | bytes accessed | tf_op | source)
XLA Modules:
  0.0 403.0 jit_solution(6448541057434318388)
XLA Ops:
  7.2 0.0 copy-start.2
  7.2 2.4 multiply_convert_fusion.1
  9.6 0.0 copy-done.2
  9.6 3.1 maximum_maximum_fusion
  12.6 0.0 copy-start.3
  12.6 12.1 %all-to-all-start = ((bf16[32,64,1536]{2,1,0:T(8,128)(2,1)}), bf16[32,64,1536]{2,1,0:T(8,128)(2,1)}, u32[]{:S(2)}, u32[]{:S(2)}) async-start(bf16[32,64,1536]{2,1,0:T(8,128)(2,1)} %maximum_maximum_fusion), calls=%async_computation | async-start | bytes 12582912 | tf_op jit(solution)/shard_map/all_to_all | solution.py:16
  24.7 0.0 copy-done.3
  24.8 0.0 copy-start.1
  24.8 0.1 copy.45
  24.9 0.2 eq.73
  25.1 0.2 eq.69
  25.3 4.5 %reduce-window.6 = s32[16,8,128]{2,1,0:T(8,128)S(1)} reduce-window(s32[16,8,128]{2,1,0:T(8,128)S(1)} %fusion.70, s32[]{:T(128)} %constant.8.clone.1), window={size=1x1x128 pad=0_0x0_0x127_0}, to_apply=%region_0.0 | reduce-window | flops 2080768 | bytes 131076 | tf_op jit(solution)/shard_map/reduce-window
  29.8 0.1 slice.32
  29.9 0.1 copy.47
  30.0 0.1 copy.48
  30.1 0.1 broadcast_add_fusion
  30.2 0.2 reduce_sum.21
  30.5 0.1 copy.49
  30.6 2.0 fusion
  32.6 0.0 copy-done.1
  32.6 0.5 fusion.1
  33.1 3.8 convolution_convert_fusion
  36.9 3.2 fusion.74
  40.1 121.7 %all-to-all-done = bf16[32,64,1536]{2,1,0:T(8,128)(2,1)} async-done(((bf16[32,64,1536]{2,1,0:T(8,128)(2,1)}), bf16[32,64,1536]{2,1,0:T(8,128)(2,1)}, u32[]{:S(2)}, u32[]{:S(2)}) %all-to-all-start) | async-done | bytes 6291488 | tf_op jit(solution)/shard_map/all_to_all | solution.py:16
  161.8 15.1 %all-to-all-start.2 = ((bf16[16,1,48,2048]{3,2,1,0:T(8,128)(2,1)}), bf16[16,1,48,2048]{3,2,1,0:T(8,128)(2,1)S(1)}, u32[]{:S(2)}, u32[]{:S(2)}) async-start(bf16[16,1,48,2048]{3,2,1,0:T(8,128)(2,1)} %get-tuple-element.5), calls=%async_computation.3 | async-start | bytes 6291456 | tf_op jit(solution)/shard_map/all_to_all | solution.py:33
  176.9 5.7 %fusion.75 = (bf16[1,2048,512]{2,1,0:T(8,128)(2,1)}, bf16[1,2048,512]{2,1,0:T(8,128)(2,1)}, bf16[1,2048,512]{2,1,0:T(8,128)(2,1)}) fusion(bf16[1,2048,1536]{2,1,0:T(8,128)(2,1)} %bitcast), kind=kLoop, calls=%fused_computation.72 | loop fusion | bytes 12582912 | tf_op jit(solution)/shard_map/split | solution.py:17
  182.7 54.2 %all-to-all-done.2 = bf16[16,1,48,2048]{3,2,1,0:T(8,128)(2,1)S(1)} async-done(((bf16[16,1,48,2048]{3,2,1,0:T(8,128)(2,1)}), bf16[16,1,48,2048]{3,2,1,0:T(8,128)(2,1)S(1)}, u32[]{:S(2)}, u32[]{:S(2)}) %all-to-all-start.2) | async-done | bytes 3145760 | tf_op jit(solution)/shard_map/all_to_all | solution.py:33
  236.8 0.0 copy-start
  236.8 1.7 copy-done
  238.5 15.3 %all-to-all-start.1 = ((bf16[16,1,48,2048]{3,2,1,0:T(8,128)(2,1)}), bf16[16,1,48,2048]{3,2,1,0:T(8,128)(2,1)S(1)}, u32[]{:S(2)}, u32[]{:S(2)}) async-start(bf16[16,1,48,2048]{3,2,1,0:T(8,128)(2,1)} %get-tuple-element.4), calls=%async_computation.1 | async-start | bytes 6291456 | tf_op jit(solution)/shard_map/all_to_all | solution.py:33
  253.8 0.0 reduce-scatter.5.cloned.1.call-start
  253.8 5.5 %fusion.3 = f32[512,16,48]{0,2,1:T(8,128)} fusion(bf16[16,1,48,2048]{3,2,1,0:T(8,128)(2,1)} %copy-done, bf16[1,2048,512]{2,1,0:T(8,128)(2,1)} %get-tuple-element.7), kind=kOutput, calls=%fused_computation.10 | convolution fusion | flops 1610612736 | bytes 6815744 | tf_op jit(solution)/shard_map/sjnd,jdf->sjnf/dot_general | solution.py:71
  259.3 8.8 %fusion.16 = bf16[16,1,48,2048]{3,2,0,1:T(8,128)(2,1)} fusion(bf16[1,2048,512]{2,1,0:T(8,128)(2,1)} %get-tuple-element.6, f32[512,16,48]{0,2,1:T(8,128)} %fusion.3, bf16[16,1,48,2048]{3,2,1,0:T(8,128)(2,1)} %copy-done, bf16[1,2048,512]{2,1,0:T(8,128)(2,1)} %get-tuple-element.8), kind=kOutput, calls=%fused_computation.25 | convolution fusion | flops 3225157632 | bytes 12058624 | tf_op jit(solution)/shard_map/sjnf,jdf->sjnd/dot_general | solution.py:73
  268.1 0.0 reduce-scatter.5.cloned.1.call-update
  268.1 0.2 reduce-scatter.3.cloned.1.call-start
  268.3 45.4 %all-to-all-done.1 = bf16[16,1,48,2048]{3,2,1,0:T(8,128)(2,1)S(1)} async-done(((bf16[16,1,48,2048]{3,2,1,0:T(8,128)(2,1)}), bf16[16,1,48,2048]{3,2,1,0:T(8,128)(2,1)S(1)}, u32[]{:S(2)}, u32[]{:S(2)}) %all-to-all-start.1) | async-done | bytes 3145760 | tf_op jit(solution)/shard_map/all_to_all | solution.py:33
  313.7 4.5 %fusion.7 = f32[512,16,48]{0,2,1:T(8,128)} fusion(bf16[16,1,48,2048]{3,2,1,0:T(8,128)(2,1)S(1)} %all-to-all-done.1, bf16[1,2048,512]{2,1,0:T(8,128)(2,1)} %get-tuple-element.7), kind=kOutput, calls=%fused_computation.14 | convolution fusion | flops 1610612736 | bytes 6815744 | tf_op jit(solution)/shard_map/sjnd,jdf->sjnf/dot_general | solution.py:71
  318.2 7.9 %fusion.15 = bf16[16,1,48,2048]{3,2,0,1:T(8,128)(2,1)} fusion(bf16[1,2048,512]{2,1,0:T(8,128)(2,1)} %get-tuple-element.6, f32[512,16,48]{0,2,1:T(8,128)} %fusion.7, bf16[16,1,48,2048]{3,2,1,0:T(8,128)(2,1)S(1)} %all-to-all-done.1, bf16[1,2048,512]{2,1,0:T(8,128)(2,1)} %get-tuple-element.8), kind=kOutput, calls=%fused_computation.24 | convolution fusion | flops 3225157632 | bytes 12058624 | tf_op jit(solution)/shard_map/sjnf,jdf->sjnd/dot_general | solution.py:73
  326.1 0.0 copy-start.4
  326.1 0.0 reduce-scatter.3.cloned.1.call-update
  326.2 0.0 reduce-scatter.5.cloned.1.call-done
  326.2 44.2 %reduce-scatter.3.cloned.1.call-done = bf16[16,1,48,256]{3,2,0,1:T(8,128)(2,1)} async-done(((bf16[16,1,48,2048]{3,2,0,1:T(8,128)(2,1)}), bf16[16,1,48,256]{3,2,0,1:T(8,128)(2,1)}) %reduce-scatter.3.cloned.1.call-update) | async-done | bytes 393232 | tf_op jit(solution)/shard_map/reduce_scatter | solution.py:77
  370.4 2.1 maximum_bitcast_fusion
  372.5 6.7 %all-to-all-start.3 = ((bf16[16,1,96,256]{3,2,1,0:T(8,128)(2,1)}), bf16[16,1,96,256]{3,2,1,0:T(8,128)(2,1)S(1)}, u32[]{:S(2)}, u32[]{:S(2)}) async-start(bf16[16,1,96,256]{3,2,1,0:T(8,128)(2,1)} %maximum_bitcast_fusion), calls=%async_computation.5 | async-start | bytes 1572864 | tf_op jit(solution)/shard_map/all_to_all | solution.py:83
  379.2 0.0 copy-done.4
  379.2 15.3 %all-to-all-done.3 = bf16[16,1,96,256]{3,2,1,0:T(8,128)(2,1)S(1)} async-done(((bf16[16,1,96,256]{3,2,1,0:T(8,128)(2,1)}), bf16[16,1,96,256]{3,2,1,0:T(8,128)(2,1)S(1)}, u32[]{:S(2)}, u32[]{:S(2)}) %all-to-all-start.3) | async-done | bytes 786464 | tf_op jit(solution)/shard_map/all_to_all | solution.py:83
  394.5 1.7 fusion.56
  (8 shorter events, 0.1 us)
Async XLA Ops:
  7.2 2.4 copy-start.2
  12.6 12.1 %copy-start.3 = (s32[512,2]{0,1:T(2,128)S(1)}, s32[512,2]{0,1:T(2,128)}, u32[]{:S(2)}) copy-start(s32[512,2]{0,1:T(2,128)} %param.8) | copy-start | bytes 12292
  12.6 149.2 %all-to-all-start = ((bf16[32,64,1536]{2,1,0:T(8,128)(2,1)}), bf16[32,64,1536]{2,1,0:T(8,128)(2,1)}, u32[]{:S(2)}, u32[]{:S(2)}) async-start(bf16[32,64,1536]{2,1,0:T(8,128)(2,1)} %maximum_maximum_fusion), calls=%async_computation | async-start | bytes 12582912 | tf_op jit(solution)/shard_map/all_to_all | solution.py:16
  24.8 7.8 %copy-start.1 = (bf16[512,2048]{1,0:T(8,128)(2,1)S(1)}, bf16[512,2048]{1,0:T(8,128)(2,1)}, u32[]{:S(2)}) copy-start(bf16[512,2048]{1,0:T(8,128)(2,1)} %param.7) | copy-start | bytes 6291460
  161.8 75.0 %all-to-all-start.2 = ((bf16[16,1,48,2048]{3,2,1,0:T(8,128)(2,1)}), bf16[16,1,48,2048]{3,2,1,0:T(8,128)(2,1)S(1)}, u32[]{:S(2)}, u32[]{:S(2)}) async-start(bf16[16,1,48,2048]{3,2,1,0:T(8,128)(2,1)} %get-tuple-element.5), calls=%async_computation.3 | async-start | bytes 6291456 | tf_op jit(solution)/shard_map/all_to_all | solution.py:33
  236.8 1.7 copy-start
  238.5 75.2 %all-to-all-start.1 = ((bf16[16,1,48,2048]{3,2,1,0:T(8,128)(2,1)}), bf16[16,1,48,2048]{3,2,1,0:T(8,128)(2,1)S(1)}, u32[]{:S(2)}, u32[]{:S(2)}) async-start(bf16[16,1,48,2048]{3,2,1,0:T(8,128)(2,1)} %get-tuple-element.4), calls=%async_computation.1 | async-start | bytes 6291456 | tf_op jit(solution)/shard_map/all_to_all | solution.py:33
  253.8 72.4 %reduce-scatter.5.cloned.1.call-start = ((), (), s32[]{:S(2)}) async-start(), calls=%async_computation.7 | async-start | bytes 3538944 | tf_op jit(solution)/shard_map/reduce_scatter | solution.py:77
  268.1 102.4 %reduce-scatter.3.cloned.1.call-start = ((), (), s32[]{:S(2)}) async-start(), calls=%async_computation.6 | async-start | bytes 3538944 | tf_op jit(solution)/shard_map/reduce_scatter | solution.py:77
  326.1 53.1 %copy-start.4 = (f32[512,2]{0,1:T(2,128)S(1)}, f32[512,2]{0,1:T(2,128)}, u32[]{:S(2)}) copy-start(f32[512,2]{0,1:T(2,128)} %param.9) | copy-start | bytes 12292
  372.5 22.0 %all-to-all-start.3 = ((bf16[16,1,96,256]{3,2,1,0:T(8,128)(2,1)}), bf16[16,1,96,256]{3,2,1,0:T(8,128)(2,1)S(1)}, u32[]{:S(2)}, u32[]{:S(2)}) async-start(bf16[16,1,96,256]{3,2,1,0:T(8,128)(2,1)} %maximum_bitcast_fusion), calls=%async_computation.5 | async-start | bytes 1572864 | tf_op jit(solution)/shard_map/all_to_all | solution.py:83
Sparse Core Ops, SparseCore 0:
  268.2 36.7 reduce-scatter.4
  326.3 44.1 reduce-scatter.2
where the time goes:
time: 408 us; the launch traced here: 403 us
  waiting for transfers between devices  281 us (69%)
  starting transfers between devices  49.4 us (12%)
  matrix products  32.2 us (8%)
  other arithmetic  14.7 us (4%)
  between operations  14.2 us (3%)
  local copies, waits for them, and re-layouts  11.6 us (3%)
    all_to_all x1, waiting for transfers between devices, sent_together(): lax.all_to_all(both, axis, split_axis=split_dim, concat_axis=concat_dim,...  122 us
    all_to_all x2, waiting for transfers between devices, grouped_exchange(): lax.all_to_all(group, axis, split_axis=split_dim, concat_axis=concat_dim,...  99.6 us
    reduce_scatter x2, waiting for transfers between devices, expert_work(): lax.psum_scatter(rounded.astype(jnp.float32).astype(jnp.bfloat16), 'tp',...  44.3 us
    all_to_all x2, starting transfers between devices, grouped_exchange(): lax.all_to_all(group, axis, split_axis=split_dim, concat_axis=concat_dim,...  30.4 us
    dot_general x2, matrix products, expert_work(): jnp.einsum('sjnf,jdf->sjnd', hidden, down_out, preferred_element_type=jnp...  16.7 us
    all_to_all x1, waiting for transfers between devices, body(): lax.all_to_all(results, 'fs', split_axis=0, concat_axis=0, tiled=True)  15.3 us
    all_to_all x1, starting transfers between devices, sent_together(): lax.all_to_all(both, axis, split_axis=split_dim, concat_axis=concat_dim,...  12.1 us
    dot_general x2, matrix products, expert_work(): jnp.einsum('sjnd,jdf->sjnf', arrived, up_out, preferred_element_type=jnp....  9.97 us
  transfers between devices with their start and end apart: 6, of which 5 were waited for; matrix products, arithmetic and copies ran while one was open for 12% of the time, Pallas kernels for 0%

commit v1 on v0

--- a/solution.py
+++ b/solution.py
@@ -17,27 +17,6 @@
     return tuple(jnp.split(whole, [sum(widths[:k]) for k in range(1, len(widths))], axis=along))
 
 
-def grouped_exchange(value, axis, split_dim, concat_dim, work, item_dim, out_dim):
-    items = jax.tree.leaves(value)[0].shape[item_dim]
-    count = 2 if items % 2 == 0 else 1
-    outs = []
-    for k in range(count):
-        group = jax.tree.map(
-            lambda a: lax.slice_in_dim(
-                a, k * (items // count), (k + 1) * (items // count), axis=item_dim
-            ),
-            value,
-        )
-        outs.append(
-            work(
-                lax.all_to_all(
-                    group, axis, split_axis=split_dim, concat_axis=concat_dim, tiled=True
-                )
-            )
-        )
-    return jax.tree.map(lambda *parts: jnp.concatenate(parts, axis=out_dim), *outs)
-
-
 def body(tokens, routes, route_weight, gain, w_gate, w_up, w_down):
     scaling = gain[None, :, None]
     gate_local = (w_gate * scaling).astype(jnp.bfloat16)
@@ -45,9 +24,6 @@
     gate_twice = jnp.concatenate([gate_local, gate_local], axis=0)
     up_twice = jnp.concatenate([up_local, up_local], axis=0)
     down_twice = jnp.concatenate([w_down, w_down], axis=0)
-    gate_out, up_out, down_out = sent_together(
-        (gate_twice, up_twice, down_twice), ("gr", "fs"), 0, 1, 2
-    )
     fs_count = lax.axis_size("fs")
     experts = EXP_DEV * fs_count
     tok_rows = tokens.shape[0]
@@ -63,8 +39,17 @@
     slot_ids = jnp.arange(experts * capacity, dtype=jnp.int32)
     hits = slot_ids[:, None, None] == destination[None, :, :]
     dispatch = jnp.any(hits, axis=-1).astype(jnp.bfloat16)
-    outgoing = jnp.dot(dispatch, normed, preferred_element_type=jnp.float32).astype(jnp.bfloat16)
-    outgoing = outgoing.reshape(fs_count, EXP_DEV, capacity, D)
+    part = D // lax.axis_size("tp")
+    mine = lax.dynamic_slice_in_dim(normed, lax.axis_index("tp") * part, part, axis=1)
+    outgoing = jnp.dot(dispatch, mine, preferred_element_type=jnp.float32).astype(jnp.bfloat16)
+    outgoing = outgoing.reshape(fs_count, EXP_DEV, capacity, part)
+    arrived = lax.all_to_all(outgoing, "fs", split_axis=0, concat_axis=0, tiled=True)
+    gate_twice, up_twice, down_twice, arrived = lax.optimization_barrier(
+        (gate_twice, up_twice, down_twice, arrived)
+    )
+    arrived = lax.all_gather(arrived, "tp", axis=3, tiled=True)
+    gate_out, up_out = sent_together((gate_twice, up_twice), ("gr", "fs"), 0, 1, 2)
+    (down_out,) = sent_together((down_twice,), ("gr", "fs"), 0, 1, 2)
 
     def expert_work(arrived):
         gate = jnp.einsum("sjnd,jdf->sjnf", arrived, gate_out, preferred_element_type=jnp.float32)
@@ -79,7 +64,7 @@
         )
         return summed
 
-    results = grouped_exchange(outgoing, "fs", 0, 0, expert_work, 2, 2)
+    results = expert_work(arrived)
     back_home = lax.all_to_all(results, "fs", split_axis=0, concat_axis=0, tiled=True)
     features = back_home.shape[-1]
     flat_back = back_home.reshape(experts * capacity, features).astype(jnp.float32)

time: 408 us -> 307 us (0.75)
  waiting for transfers between devices: 281 us -> 204 us
  starting transfers between devices: 49.4 us -> 34.2 us
  matrix products: 32.2 us -> 24.6 us
  other arithmetic: 14.7 us -> 19.9 us
    all_to_all x2 -> x1, waiting for transfers between devices: 99.6 us -> 14.2 us  [body(): lax.all_to_all(outgoing, 'fs', split_axis=0, concat_axis=0, tiled=True)]
    all_to_all x2 -> x1, starting transfers between devices: 30.4 us -> 9.13 us  [body(): lax.all_to_all(outgoing, 'fs', split_axis=0, concat_axis=0, tiled=True)]
    all_to_all x1 -> x2, starting transfers between devices: 12.1 us -> 17.8 us  [sent_together(): lax.all_to_all(both, axis, split_axis=split_dim, concat_axis=concat_dim,...]
    dot_general x2 -> x1, matrix products: 16.7 us -> 11.8 us  [expert_work(): jnp.einsum('sjnf,jdf->sjnd', hidden, down_out, preferred_element_type=jnp...]
    all_to_all x1 -> x2, waiting for transfers between devices: 122 us -> 126 us  [sent_together(): lax.all_to_all(both, axis, split_axis=split_dim, concat_axis=concat_dim,...]
    dot_general x2 -> x1, matrix products: 9.97 us -> 8.47 us  [expert_work(): jnp.einsum('sjnd,jdf->sjnf', arrived, up_out, preferred_element_type=jnp....]
    reduce_scatter x2 -> x1, waiting for transfers between devices: 44.3 us -> 44.5 us  [expert_work(): lax.psum_scatter(rounded.astype(jnp.float32).astype(jnp.bfloat16), 'tp',...]
  transfers between devices with their start and end apart: 6 -> 6, of which waited for: 5 -> 5; matrix products, arithmetic and copies ran while one was open for 12% -> 6% of each run, Pallas kernels for 0% -> 0%
where the time goes in v1:
time: 307 us; the launch traced here: 304 us
  waiting for transfers between devices  204 us (66%)
  starting transfers between devices  34.2 us (11%)
  matrix products  24.6 us (8%)
  other arithmetic  19.9 us (6%)
  between operations  14.2 us (5%)
  local copies, waits for them, and re-layouts  7.62 us (2%)
    all_to_all x2, waiting for transfers between devices, sent_together(): lax.all_to_all(both, axis, split_axis=split_dim, concat_axis=concat_dim,...  126 us
    reduce_scatter x1, waiting for transfers between devices, expert_work(): lax.psum_scatter(rounded.astype(jnp.float32).astype(jnp.bfloat16), 'tp',...  44.5 us
    all_to_all x2, starting transfers between devices, sent_together(): lax.all_to_all(both, axis, split_axis=split_dim, concat_axis=concat_dim,...  17.8 us
    all_to_all x1, waiting for transfers between devices, body(): lax.all_to_all(results, 'fs', split_axis=0, concat_axis=0, tiled=True)  17.7 us
    all_to_all x1, waiting for transfers between devices, body(): lax.all_to_all(outgoing, 'fs', split_axis=0, concat_axis=0, tiled=True)  14.2 us
    dot_general x1, matrix products, expert_work(): jnp.einsum('sjnf,jdf->sjnd', hidden, down_out, preferred_element_type=jnp...  11.8 us
    all_to_all x1, starting transfers between devices, body(): lax.all_to_all(outgoing, 'fs', split_axis=0, concat_axis=0, tiled=True)  9.13 us
    dot_general x1, matrix products, expert_work(): jnp.einsum('sjnd,jdf->sjnf', arrived, up_out, preferred_element_type=jnp....  8.47 us
  transfers between devices with their start and end apart: 6, of which 5 were waited for; matrix products, arithmetic and copies ran while one was open for 6% of the time, Pallas kernels for 0%

profile of v1, /device:TPU:1, one launch (start us, length us, event | category | flops | bytes accessed | tf_op | source)
XLA Modules:
  0.0 304.1 jit_solution(14894455003133973554)
XLA Ops:
  7.2 0.8 copy.45
  8.0 0.2 eq.73
  8.2 0.2 eq.69
  8.3 0.0 copy-start
  8.4 4.2 %convert_element_type.53 = f32[512,2048]{1,0:T(8,128)} convert(bf16[512,2048]{1,0:T(8,128)(2,1)} %param.7) | non-fusion elementwise | flops 1048576 | bytes 6291456 | tf_op jit(solution)/shard_map/convert_element_type | solution.py:31
  12.6 0.0 copy-done
  12.6 0.0 copy-start.5
  12.6 0.5 multiply_reduce_fusion
  13.1 4.5 %reduce-window.6 = s32[16,8,128]{2,1,0:T(8,128)S(1)} reduce-window(s32[16,8,128]{2,1,0:T(8,128)S(1)} %fusion.42, s32[]{:T(128)} %constant.6.clone.1), window={size=1x1x128 pad=0_0x0_0x127_0}, to_apply=%region_0.0 | reduce-window | flops 2080768 | bytes 131076 | tf_op jit(solution)/shard_map/reduce-window
  17.6 0.1 slice.24
  17.7 0.1 copy.47
  17.8 0.1 copy.48
  17.9 0.1 broadcast_add_fusion
  18.0 0.2 reduce_sum.21
  18.2 0.0 copy-start.2
  18.3 0.1 copy.49
  18.4 0.0 copy-done.5
  18.4 2.0 fusion.4
  20.4 2.6 convolution_convert_fusion
  23.0 9.1 %all-to-all-start = ((bf16[16,1,96,256]{3,2,1,0:T(8,128)(2,1)}), bf16[16,1,96,256]{3,2,1,0:T(8,128)(2,1)S(1)}, u32[]{:S(2)}, u32[]{:S(2)}) async-start(bf16[16,1,96,256]{3,2,1,0:T(8,128)(2,1)} %bitcast.101), calls=%async_computation | async-start | bytes 1572864 | tf_op jit(solution)/shard_map/all_to_all | solution.py:46
  32.2 0.0 copy-done.2
  32.2 0.0 copy-start.4
  32.2 1.5 pad_maximum_fusion.3
  33.7 0.0 copy-done.3
  33.7 0.0 copy-done.7
  33.7 0.0 copy-done.4
  33.7 0.7 multiply_convert_fusion
  34.4 1.7 pad_maximum_fusion.1
  36.1 14.2 %all-to-all-done = bf16[16,1,96,256]{3,2,1,0:T(8,128)(2,1)S(1)} async-done(((bf16[16,1,96,256]{3,2,1,0:T(8,128)(2,1)}), bf16[16,1,96,256]{3,2,1,0:T(8,128)(2,1)S(1)}, u32[]{:S(2)}, u32[]{:S(2)}) %all-to-all-start) | async-done | bytes 786464 | tf_op jit(solution)/shard_map/all_to_all | solution.py:46
  50.3 4.6 %pad_maximum_fusion = bf16[32,64,1024]{2,1,0:T(8,128)(2,1)} fusion(bf16[32,64,512]{2,1,0:T(8,128)(2,1)} %get-tuple-element.9, bf16[32,64,512]{2,1,0:T(8,128)(2,1)S(1)} %get-tuple-element.8), kind=kLoop, calls=%fused_computation.7 | loop fusion | flops 8388608 | bytes 8388608 | tf_op jit(solution)/shard_map/concatenate | solution.py:15
  54.9 0.0 copy-done.1
  54.9 9.6 %all-to-all-start.1 = ((bf16[32,64,1024]{2,1,0:T(8,128)(2,1)}), bf16[32,64,1024]{2,1,0:T(8,128)(2,1)}, u32[]{:S(2)}, u32[]{:S(2)}) async-start(bf16[32,64,1024]{2,1,0:T(8,128)(2,1)} %pad_maximum_fusion), calls=%async_computation.1 | async-start | bytes 8388608 | tf_op jit(solution)/shard_map/all_to_all | solution.py:16
  64.5 0.0 all-gather.2.cloned.1.call-start
  64.5 0.7 all-gather.2.cloned.1.call-update
  65.2 91.5 %all-to-all-done.1 = bf16[32,64,1024]{2,1,0:T(8,128)(2,1)} async-done(((bf16[32,64,1024]{2,1,0:T(8,128)(2,1)}), bf16[32,64,1024]{2,1,0:T(8,128)(2,1)}, u32[]{:S(2)}, u32[]{:S(2)}) %all-to-all-start.1) | async-done | bytes 4194336 | tf_op jit(solution)/shard_map/all_to_all | solution.py:16
  156.7 8.2 %all-to-all-start.2 = ((bf16[32,64,512]{2,1,0:T(8,128)(2,1)}), bf16[32,64,512]{2,1,0:T(8,128)(2,1)S(1)}, u32[]{:S(2)}, u32[]{:S(2)}) async-start(bf16[32,64,512]{2,1,0:T(8,128)(2,1)} %pad_maximum_fusion.3), calls=%async_computation.2 | async-start | bytes 4194304 | tf_op jit(solution)/shard_map/all_to_all | solution.py:16
  164.9 0.2 reduce-scatter.2.cloned.1.call-start
  165.1 4.5 %fusion.46 = (bf16[1,2048,512]{2,1,0:T(8,128)(2,1)}, bf16[1,2048,512]{2,1,0:T(8,128)(2,1)}) fusion(bf16[1,2048,1024]{2,1,0:T(8,128)(2,1)} %bitcast.4), kind=kLoop, calls=%fused_computation.53 | loop fusion | bytes 8388608 | tf_op jit(solution)/shard_map/split | solution.py:17
  169.6 8.5 %fusion = f32[512,16,96]{0,2,1:T(8,128)} fusion(bf16[16,1,96,2048]{3,2,0,1:T(8,128)(2,1)} %all-gather.2.cloned.1.call-done, bf16[1,2048,512]{2,1,0:T(8,128)(2,1)} %get-tuple-element.27), kind=kOutput, calls=%fused_computation | convolution fusion | flops 3221225472 | bytes 11534336 | tf_op jit(solution)/shard_map/sjnd,jdf->sjnf/dot_general | solution.py:56
  178.1 35.0 %all-to-all-done.2 = bf16[32,64,512]{2,1,0:T(8,128)(2,1)S(1)} async-done(((bf16[32,64,512]{2,1,0:T(8,128)(2,1)}), bf16[32,64,512]{2,1,0:T(8,128)(2,1)S(1)}, u32[]{:S(2)}, u32[]{:S(2)}) %all-to-all-start.2) | async-done | bytes 2097184 | tf_op jit(solution)/shard_map/all_to_all | solution.py:16
  213.0 11.8 %convert_bitcast_fusion = bf16[16,1,96,2048]{3,2,0,1:T(8,128)(2,1)} fusion(bf16[2048,512,1]{1,0,2:T(8,128)(2,1)S(1)} %bitcast.97, f32[512,16,96]{0,2,1:T(8,128)} %fusion, bf16[16,1,96,2048]{3,2,0,1:T(8,128)(2,1)} %all-gather.2.cloned.1.call-done, bf16[1,2048,512]{2,1,0:T(8,128)(2,1)} %get-tuple-element.26), kind=kOutput, calls=%fused_computation.4 | convolution fusion | flops 6450315264 | bytes 19922944 | tf_op jit(solution)/shard_map/sjnf,jdf->sjnd/dot_general | solution.py:58
  224.9 0.0 reduce-scatter.2.cloned.1.call-update
  224.9 44.5 %reduce-scatter.2.cloned.1.call-done = bf16[16,1,96,256]{3,2,0,1:T(8,128)(2,1)} async-done(((bf16[16,1,96,2048]{3,2,0,1:T(8,128)(2,1)}), bf16[16,1,96,256]{3,2,0,1:T(8,128)(2,1)}) %reduce-scatter.2.cloned.1.call-update) | async-done | bytes 786448 | tf_op jit(solution)/shard_map/reduce_scatter | solution.py:62
  269.4 7.0 %all-to-all-start.3 = ((bf16[16,1,96,256]{3,2,1,0:T(8,128)(2,1)}), bf16[16,1,96,256]{3,2,1,0:T(8,128)(2,1)S(1)}, u32[]{:S(2)}, u32[]{:S(2)}) async-start(bf16[16,1,96,256]{3,2,1,0:T(8,128)(2,1)} %bitcast.100), calls=%async_computation.4 | async-start | bytes 1572864 | tf_op jit(solution)/shard_map/all_to_all | solution.py:68
  276.5 0.0 copy-done.6
  276.5 17.7 %all-to-all-done.3 = bf16[16,1,96,256]{3,2,1,0:T(8,128)(2,1)S(1)} async-done(((bf16[16,1,96,256]{3,2,1,0:T(8,128)(2,1)}), bf16[16,1,96,256]{3,2,1,0:T(8,128)(2,1)S(1)}, u32[]{:S(2)}, u32[]{:S(2)}) %all-to-all-start.3) | async-done | bytes 786464 | tf_op jit(solution)/shard_map/all_to_all | solution.py:68
  294.2 1.7 fusion.25
  295.9 1.3 copy.56
  (13 shorter events, 0.1 us)
Async XLA Ops:
  8.3 4.2 %copy-start = (bf16[512,2048]{1,0:T(8,128)(2,1)S(1)}, bf16[512,2048]{1,0:T(8,128)(2,1)}, u32[]{:S(2)}) copy-start(bf16[512,2048]{1,0:T(8,128)(2,1)} %param.7) | copy-start | bytes 6291460
  12.6 5.8 %copy-start.5 = (s32[512,2]{0,1:T(2,128)S(1)}, s32[512,2]{0,1:T(2,128)}, u32[]{:S(2)}) copy-start(s32[512,2]{0,1:T(2,128)} %param.8) | copy-start | bytes 12292
  18.2 13.9 %copy-start.2 = (bf16[16,64,512]{2,1,0:T(8,128)(2,1)S(1)}, bf16[16,64,512]{2,1,0:T(8,128)(2,1)}, u32[]{:S(2)}) copy-start(bf16[16,64,512]{2,1,0:T(8,128)(2,1)} %param.13) | copy-start | bytes 3145732
  23.0 10.6 %copy-start.3 = (bf16[16,64,512]{2,1,0:T(8,128)(2,1)S(1)}, bf16[16,64,512]{2,1,0:T(8,128)(2,1)}, u32[]{:S(2)}) copy-start(bf16[16,64,512]{2,1,0:T(8,128)(2,1)} %param.12) | copy-start | bytes 3145732
  23.0 10.6 %copy-start.7 = (f32[64]{0:T(128)S(1)}, f32[64]{0:T(128)}, u32[]{:S(2)}) copy-start(f32[64]{0:T(128)} %param.10) | copy-start | bytes 772
  23.0 27.3 %all-to-all-start = ((bf16[16,1,96,256]{3,2,1,0:T(8,128)(2,1)}), bf16[16,1,96,256]{3,2,1,0:T(8,128)(2,1)S(1)}, u32[]{:S(2)}, u32[]{:S(2)}) async-start(bf16[16,1,96,256]{3,2,1,0:T(8,128)(2,1)} %bitcast.101), calls=%async_computation | async-start | bytes 1572864 | tf_op jit(solution)/shard_map/all_to_all | solution.py:46
  32.2 1.5 copy-start.4
  50.3 4.6 %copy-start.1 = (bf16[16,1,96,256]{3,2,1,0:T(8,128)(2,1)}, bf16[16,1,96,256]{3,2,1,0:T(8,128)(2,1)S(1)}, u32[]{:S(2)}) copy-start(bf16[16,1,96,256]{3,2,1,0:T(8,128)(2,1)S(1)} %all-to-all-done) | copy-start | bytes 2359300
  54.9 101.8 %all-to-all-start.1 = ((bf16[32,64,1024]{2,1,0:T(8,128)(2,1)}), bf16[32,64,1024]{2,1,0:T(8,128)(2,1)}, u32[]{:S(2)}, u32[]{:S(2)}) async-start(bf16[32,64,1024]{2,1,0:T(8,128)(2,1)} %pad_maximum_fusion), calls=%async_computation.1 | async-start | bytes 8388608 | tf_op jit(solution)/shard_map/all_to_all | solution.py:16
  64.5 105.1 %all-gather.2.cloned.1.call-start = ((), (), s32[]{:S(2)}) async-start(), calls=%async_computation.5 | async-start | bytes 7077888 | tf_op jit(solution)/shard_map/all_gather | solution.py:50
  156.7 56.3 %all-to-all-start.2 = ((bf16[32,64,512]{2,1,0:T(8,128)(2,1)}), bf16[32,64,512]{2,1,0:T(8,128)(2,1)S(1)}, u32[]{:S(2)}, u32[]{:S(2)}) async-start(bf16[32,64,512]{2,1,0:T(8,128)(2,1)} %pad_maximum_fusion.3), calls=%async_computation.2 | async-start | bytes 4194304 | tf_op jit(solution)/shard_map/all_to_all | solution.py:16
  164.9 104.6 %reduce-scatter.2.cloned.1.call-start = ((), (), s32[]{:S(2)}) async-start(), calls=%async_computation.6 | async-start | bytes 7077888 | tf_op jit(solution)/shard_map/reduce_scatter | solution.py:62
  224.9 51.6 %copy-start.6 = (f32[512,2]{0,1:T(2,128)S(1)}, f32[512,2]{0,1:T(2,128)}, u32[]{:S(2)}) copy-start(f32[512,2]{0,1:T(2,128)} %param.9) | copy-start | bytes 12292
  269.4 24.8 %all-to-all-start.3 = ((bf16[16,1,96,256]{3,2,1,0:T(8,128)(2,1)}), bf16[16,1,96,256]{3,2,1,0:T(8,128)(2,1)S(1)}, u32[]{:S(2)}, u32[]{:S(2)}) async-start(bf16[16,1,96,256]{3,2,1,0:T(8,128)(2,1)} %bitcast.100), calls=%async_computation.4 | async-start | bytes 1572864 | tf_op jit(solution)/shard_map/all_to_all | solution.py:68
Sparse Core Ops, SparseCore 0:
  67.1 49.7 all-gather.1
  225.0 44.3 reduce-scatter.1

commit v2 on v1

v2 whole, which is shorter than its diff:
```python
import functools

import jax
import jax.numpy as jnp
from jax import lax
from jax.experimental import pallas as pl
from jax.experimental.pallas import tpu as pltpu
from jax.sharding import PartitionSpec as P

MESH = pl.DeviceIdType.MESH
F32, BF16 = jnp.float32, jnp.bfloat16
EPSILON = 1e-05
D, UNITS, EXPERTS, TOK, CAP, TP, SOURCES = 2048, 512, 16, 512, 96, 8, 32
PART = D // TP
ROWS = EXPERTS * CAP
ROUNDS, HALF = 2, 128


def iota(shape, axis):
    return lax.broadcasted_iota(jnp.int32, shape, axis)


def kernel(
    tok_hbm, routes_ref, weight_ref, gain_ref, wg_hbm, wu_hbm, wd_hbm,
    go_hbm, uo_hbm, do_hbm, mixed_ref,
    tok, mine, normed, dest, cmap, gu, outgoing, gur, dn, rows, hidden,
    pair_out, pair_in, own, chip, ring_in, result, back,
    load_sem, self_sem, store_sem, gu_send, gu_recv, dn_send, dn_recv, tok_send, tok_recv,
    y_send, y_recv, core_send, core_recv, pair_send, pair_recv, ring_send, ring_recv, back_send, back_recv,
):
    gr, fs, tp = lax.axis_index("gr"), lax.axis_index("fs"), lax.axis_index("tp")
    z, x = gr * 4 + fs // 4, fs % 4
    y, core = tp // 2, tp % 2
    me = gr * 16 + fs
    odd = z % 2

    def plane(z2, x2):
        return {"gr": z2 // 4, "fs": (z2 % 4) * 4 + x2, "tp": tp}

    def peer(k):
        i, turn = k // 4, k % 4
        far = (i + 1) // 2
        step = (i % 2) * far + (1 - i % 2) * ((8 - far) % 8)
        return (z + step) % 8, (x + turn) % 4

    def column(y2, core2):
        return {"gr": gr, "fs": fs, "tp": y2 * 2 + core2}

    def remote(src, dst, send, recv, device):
        return pltpu.make_async_remote_copy(
            src_ref=src, dst_ref=dst, send_sem=send, recv_sem=recv, device_id=device, device_id_type=MESH
        )

    def drained(ref, sem):
        pltpu.make_async_copy(ref, ref, sem).wait()

    barrier = pltpu.get_barrier_semaphore()

    def greet(k, carry):
        pl.semaphore_signal(barrier, inc=1, device_id=plane(*peer(k)), device_id_type=MESH)
        return carry

    lax.fori_loop(1, 32, greet, 0)
    for turn in range(1, 4):
        pl.semaphore_signal(barrier, inc=1, device_id=column((y + turn) % 4, core), device_id_type=MESH)
    pl.semaphore_signal(barrier, inc=1, device_id=column(y, 1 - core), device_id_type=MESH)

    loads = [
        pltpu.make_async_copy(wg_hbm, gu.at[:, 0], load_sem.at[0]),
        pltpu.make_async_copy(wu_hbm, gu.at[:, 1], load_sem.at[1]),
        pltpu.make_async_copy(tok_hbm, tok, load_sem.at[2]),
        pltpu.make_async_copy(tok_hbm.at[:, pl.ds(pl.multiple_of(tp * PART, PART), PART)], mine, load_sem.at[3]),
    ]
    for load in loads:
        load.start()

    r0, r1 = routes_ref[0:1, :].astype(F32), routes_ref[1:2, :].astype(F32)
    names = iota((EXPERTS, TOK), 0).astype(F32)
    named = jnp.where((names == r0) | (names == r1), 1.0, 0.0)
    earlier = jnp.where(iota((TOK, TOK), 0) < iota((TOK, TOK), 1), 1.0, 0.0).astype(BF16)
    rank = jnp.dot(named.astype(BF16), earlier, preferred_element_type=F32)
    dest[0:1, :] = r0 * CAP + jnp.sum(jnp.where(names == r0, rank, 0.0), axis=0, keepdims=True)
    dest[1:2, :] = r1 * CAP + jnp.sum(jnp.where(names == r1, rank, 0.0), axis=0, keepdims=True)

    diagonal = iota((64, 64), 0) == iota((64, 64), 1)
    gain = jnp.sum(jnp.where(diagonal, gain_ref[...], 0.0), axis=1, keepdims=True)
    loads[0].wait()
    loads[1].wait()

    def scale(e, carry):
        for m in range(2):
            gu[e, m] = (gu[e, m].astype(F32) * gain).astype(BF16)
        return carry

    lax.fori_loop(0, EXPERTS, scale, 0)

    loads[2].wait()
    loads[3].wait()

    def norm(b, carry):
        at = pl.ds(pl.multiple_of(b * 64, 64), 64)
        full = tok[at, :].astype(F32)
        inverse = lax.rsqrt(jnp.mean(full * full, axis=-1, keepdims=True) + EPSILON)
        normed[at, :] = (mine[at, :].astype(F32) * inverse).astype(BF16)
        return carry

    lax.fori_loop(0, TOK // 64, norm, 0)

    def pick(e, carry):
        slot = (iota((CAP, TOK), 0) + e * CAP).astype(F32)
        hits = jnp.where((slot == dest[0:1, :]) | (slot == dest[1:2, :]), 1.0, 0.0).astype(BF16)
        outgoing[e] = jnp.dot(hits, normed[...], preferred_element_type=F32).astype(BF16)
        return carry

    lax.fori_loop(0, EXPERTS, pick, 0)

    pl.semaphore_wait(barrier, 35)

    def slot_at(z2, z1):
        return (z1 - z2 + 2 - z2 % 2 + 16) % 8

    home = slot_at(z, z) * 4 + x

    def block(slot):
        return pl.ds(pl.multiple_of(slot * CAP, CAP), CAP)

    steps = [0, 1, 7, (1 - odd) * 2 + odd * 6]
    tok_self = pltpu.make_async_copy(outgoing.at[fs], rows.at[tp, block(home)], self_sem.at[0])
    tok_self.start()
    for i in range(4):
        for turn in range(4):
            if i + turn:
                z2, x2 = (z + steps[i]) % 8, (x + turn) % 4
                remote(
                    outgoing.at[(z2 % 4) * 4 + x2], rows.at[tp, block(slot_at(z2, z) * 4 + x)],
                    tok_send, tok_recv, plane(z2, x2),
                ).start()

    gu_self = pltpu.make_async_copy(gu.at[fs], gur.at[me], self_sem.at[1])
    gu_self.start()
    dn_self = [
        pltpu.make_async_copy(wd_hbm.at[fs, pl.ds(r * 32, 32)], dn.at[r, me], self_sem.at[2 + r]) for r in range(ROUNDS)
    ]
    for copy in dn_self:
        copy.start()

    def send_gu(k, carry):
        z2, x2 = peer(k)
        remote(gu.at[(z2 % 4) * 4 + x2], gur.at[me], gu_send, gu_recv, plane(z2, x2)).start()
        return carry

    lax.fori_loop(1, 32, send_gu, 0)

    for r in range(ROUNDS):
        def send_dn(k, carry):
            z2, x2 = peer(k)
            remote(
                wd_hbm.at[(z2 % 4) * 4 + x2, pl.ds(r * 32, 32)], dn.at[r, me],
                dn_send.at[r], dn_recv.at[r], plane(z2, x2),
            ).start()
            return carry

        lax.fori_loop(1, 32, send_dn, 0)

    across = iota((TOK, TOK), 0) == iota((TOK, TOK), 1)

    def upright(row):
        return jnp.sum(jnp.where(across, row, 0.0), axis=1, keepdims=True)

    mine_cols = jnp.concatenate(
        [upright(dest[0:1, :]), upright(dest[1:2, :]), upright(weight_ref[0:1, :]), upright(weight_ref[1:2, :])], axis=1
    )
    for b in range(8):
        cols = mine_cols[b * 64 : (b + 1) * 64]
        slot = iota((64, ROWS), 1).astype(F32)
        cmap[b * 64 : (b + 1) * 64, :] = (
            jnp.where(slot == cols[:, 0:1], cols[:, 2:3], 0.0) + jnp.where(slot == cols[:, 1:2], cols[:, 3:4], 0.0)
        ).astype(BF16)

    tok_self.wait()
    drained(outgoing.at[0:15], tok_recv)
    turns = (1, 3, 2)
    y_copies = [
        remote(rows.at[tp], rows.at[tp], y_send.at[turn - 1], y_recv.at[turn - 1], column((y + turn) % 4, core))
        for turn in turns
    ]
    for copy in y_copies:
        copy.start()
    core_copies = [remote(rows.at[tp], rows.at[tp], core_send.at[0], core_recv.at[0], column(y, 1 - core))]
    core_copies[0].start()
    for turn in turns:
        origin = ((y - turn + 4) % 4) * 2 + core
        drained(rows.at[origin], y_recv.at[turn - 1])
        core_copies.append(
            remote(rows.at[origin], rows.at[origin], core_send.at[turn], core_recv.at[turn], column(y, 1 - core))
        )
        core_copies[-1].start()
    for copy in core_copies:
        copy.wait_recv()

    gu_self.wait()
    drained(gur.at[0:31], gu_recv)
    stores = [
        pltpu.make_async_copy(gur.at[:, 0], go_hbm, store_sem.at[0]),
        pltpu.make_async_copy(gur.at[:, 1], uo_hbm, store_sem.at[1]),
    ]
    for store in stores:
        store.start()

    def units(m, carry):
        at = pl.ds(pl.multiple_of(m * 512, 512), 512)
        gate, upper = jnp.zeros((512, UNITS), F32), jnp.zeros((512, UNITS), F32)
        for j in range(TP):
            lhs = rows[j, at, :]
            gate += jnp.dot(lhs, gur[4 * j : 4 * j + 4, 0].reshape(PART, UNITS), preferred_element_type=F32)
            upper += jnp.dot(lhs, gur[4 * j : 4 * j + 4, 1].reshape(PART, UNITS), preferred_element_type=F32)
        hidden[at, :] = (gate / (1.0 + jnp.exp(-gate)) * upper).astype(BF16)
        return carry

    lax.fori_loop(0, ROWS // 512, units, 0)

    pair_copies, ring_copies = [], []
    for r in range(ROUNDS):
        dn_self[r].wait()
        drained(dn.at[r, 0:31], dn_recv.at[r])
        stores.append(pltpu.make_async_copy(dn.at[r], do_hbm.at[:, pl.ds(r * 32, 32)], store_sem.at[2 + r]))
        stores[-1].start()

        def partial(parity, two, store):
            def some(m, carry):
                at = pl.ds(pl.multiple_of(m * 512, 512), 512)
                down = jnp.concatenate(
                    [
                        dn[r, pl.ds(4 * (2 * (2 * two + k) + parity), 4)].reshape(HALF, UNITS)
                        for k in range(2)
                    ],
                    axis=0,
                )
                out = lax.dot_general(
                    hidden[at, :], down, (((1,), (1,)), ((), ())), preferred_element_type=F32
                )
                for k in range(2):
                    store(2 * two + k, at, out[:, k * HALF : (k + 1) * HALF])
                return carry

            lax.fori_loop(0, ROWS // 512, some, 0)

        def give(y2, at, value):
            pair_out[r, y2, at, :] = value.astype(BF16)

        def keep(y2, at, value):
            own[r, y2, at, :] = value

        for two in range(2):
            partial(1 - core, two, give)
            for y2 in (2 * two, 2 * two + 1):
                pair_copies.append(
                    remote(
                        pair_out.at[r, y2], pair_in.at[r, y2], pair_send.at[r, y2], pair_recv.at[r, y2],
                        column(y, 1 - core),
                    )
                )
                pair_copies[-1].start()
        for two in range(2):
            partial(core, two, keep)
        for y2 in range(4):
            pair_copies[4 * r + y2].wait_recv()
        for turn in (1, 3, 2, 0):
            y2 = (y + turn) % 4

            def both(m, carry):
                at = pl.ds(pl.multiple_of(m * 256, 256), 256)
                chip[r, y2, at, :] = (own[r, y2, at, :] + pair_in[r, y2, at, :].astype(F32)).astype(BF16)
                return carry

            lax.fori_loop(0, ROWS // 256, both, 0)
            if turn:
                ring_copies.append(
                    remote(
                        chip.at[r, y2], ring_in.at[r, turn - 1], ring_send.at[r, turn - 1], ring_recv.at[r, turn - 1],
                        column(y2, core),
                    )
                )
                ring_copies[-1].start()
        for copy in ring_copies[3 * r :]:
            copy.wait_recv()

        def total(m, carry):
            at = pl.ds(pl.multiple_of(m * 256, 256), 256)
            value = chip[r, y, at, :].astype(F32)
            for turn in range(3):
                value += ring_in[r, turn, at, :].astype(F32)
            result[r, at, :] = value.astype(BF16)
            return carry

        lax.fori_loop(0, ROWS // 256, total, 0)

        stores.append(pltpu.make_async_copy(result.at[r, block(home)], back.at[r, fs], self_sem.at[4 + r]))
        stores[-1].start()
        backs = [0, 1, 7, (1 - odd) * 6 + odd * 2]
        for i in (3, 1, 2, 0):
            for turn in range(4):
                if i + turn:
                    z1, x1 = (z + backs[i]) % 8, (x + turn) % 4
                    remote(
                        result.at[r, block(slot_at(z, z1) * 4 + x1)], back.at[r, fs],
                        back_send.at[r], back_recv.at[r], plane(z1, x1),
                    ).start()

    for store in stores:
        store.wait()
    mixes = []
    for r in range(ROUNDS):
        drained(back.at[r, 0:15], back_recv.at[r])
        mixes.append(jnp.dot(cmap[...], back[r].reshape(ROWS, HALF), preferred_element_type=F32).astype(BF16))
    mixed = jnp.concatenate(mixes, axis=1)
    a, b = iota((PART, PART), 0), iota((PART, PART), 1)
    order = jnp.where((a % HALF) // 32 * 64 + a // HALF * 32 + a % 32 == b, 1.0, 0.0).astype(BF16)
    mixed_ref[...] = jnp.dot(mixed, order, preferred_element_type=F32).astype(BF16)

    drained(outgoing.at[0:15], tok_send)
    drained(gur.at[0:31], gu_send)
    for r in range(ROUNDS):
        drained(dn.at[r, 0:31], dn_send.at[r])
        drained(back.at[r, 0:15], back_send.at[r])
    for copy in y_copies + core_copies + pair_copies + ring_copies:
        copy.wait_send()


def body(tokens, routes, route_weight, gain, w_gate, w_up, w_down):
    anywhere = pl.BlockSpec(memory_space=pl.ANY)
    vmem = pl.BlockSpec(memory_space=pltpu.VMEM)
    weights = jax.ShapeDtypeStruct((SOURCES, 64, UNITS), BF16)
    dma = pltpu.SemaphoreType.DMA
    gate_out, up_out, down_out, mixed = pl.pallas_call(
        kernel,
        out_shape=(weights, weights, weights, jax.ShapeDtypeStruct((TOK, PART), BF16)),
        in_specs=[anywhere, vmem, vmem, vmem, anywhere, anywhere, anywhere],
        out_specs=(anywhere, anywhere, anywhere, vmem),
        scratch_shapes=[
            pltpu.VMEM((TOK, D), BF16),
            pltpu.VMEM((TOK, PART), BF16),
            pltpu.VMEM((TOK, PART), BF16),
            pltpu.VMEM((2, TOK), F32),
            pltpu.VMEM((TOK, ROWS), BF16),
            pltpu.VMEM((EXPERTS, 2, 64, UNITS), BF16),
            pltpu.VMEM((EXPERTS, CAP, PART), BF16),
            pltpu.VMEM((SOURCES, 2, 64, UNITS), BF16),
            pltpu.VMEM((ROUNDS, SOURCES, 32, UNITS), BF16),
            pltpu.VMEM((TP, ROWS, PART), BF16),
            pltpu.VMEM((ROWS, UNITS), BF16),
            pltpu.VMEM((ROUNDS, 4, ROWS, HALF), BF16),
            pltpu.VMEM((ROUNDS, 4, ROWS, HALF), BF16),
            pltpu.VMEM((ROUNDS, 4, ROWS, HALF), F32),
            pltpu.VMEM((ROUNDS, 4, ROWS, HALF), BF16),
            pltpu.VMEM((ROUNDS, 3, ROWS, HALF), BF16),
            pltpu.VMEM((ROUNDS, ROWS, HALF), BF16),
            pltpu.VMEM((ROUNDS, EXPERTS, CAP, HALF), BF16),
            dma((4,)),
            dma((6,)),
            dma((4,)),
            dma, dma,
            dma((ROUNDS,)), dma((ROUNDS,)),
            dma, dma,
            dma((3,)), dma((3,)),
            dma((4,)), dma((4,)),
            dma((ROUNDS, 4)), dma((ROUNDS, 4)),
            dma((ROUNDS, 3)), dma((ROUNDS, 3)),
            dma((ROUNDS,)), dma((ROUNDS,)),
        ],
        compiler_params=pltpu.CompilerParams(
            collective_id=0, has_side_effects=True, vmem_limit_bytes=60 * 1024 * 1024
        ),
    )(tokens, routes.T, route_weight.T, gain.reshape(1, -1), w_gate, w_up, w_down)
    return tuple(w.reshape(1, D, UNITS) for w in (gate_out, up_out, down_out)) + (mixed,)


def solution(mesh):
    rows = ("gr", "fs")
    weights = P(None, rows, "tp")
    placed = P("fs", None, "tp")
    return jax.shard_map(
        body,
        mesh=mesh,
        in_specs=(P(rows, None), P(rows, None), P(rows, None), P(rows), weights, weights, weights),
        out_specs=(placed, placed, placed, P(rows, "tp")),
        check_vma=False,
    )
```

time: 307 us -> 212 us (0.69)
  waiting for transfers between devices: 204 us -> 0 us
  Pallas kernels: 0 us -> 203 us
  starting transfers between devices: 34.2 us -> 0 us
  matrix products: 24.6 us -> 0 us
  other arithmetic: 19.9 us -> 0 us
  between operations: 14.2 us -> 0.65 us
    pallas_call x0 -> x1, Pallas kernels: none -> 203 us  [body(): pl.pallas_call(kernel, out_shape=(weights, weights, weights, jax.ShapeDty...]
    all_to_all x4 -> x0, waiting for transfers between devices: 158 us -> none  [the longest x2 126 us: sent_together(): lax.all_to_all(both, axis, split_axis=split_dim, concat_axis=concat_dim,...]
    reduce_scatter x1 -> x0, waiting for transfers between devices: 44.5 us -> none  [expert_work(): lax.psum_scatter(rounded.astype(jnp.float32).astype(jnp.bfloat16), 'tp',...]
    all_to_all x4 -> x0, starting transfers between devices: 33.9 us -> none  [the longest x2 17.8 us: sent_together(): lax.all_to_all(both, axis, split_axis=split_dim, concat_axis=concat_dim,...]
    dot_general x4 -> x0, matrix products: 24.6 us -> none  [the longest x1 11.8 us: expert_work(): jnp.einsum('sjnf,jdf->sjnd', hidden, down_out, preferred_element_type=jnp...]
    concatenate x3 -> x0, other arithmetic: 7.77 us -> none  [the longest x1 4.6 us: sent_together(): both = jnp.concatenate(arrays, axis=along)]
    unnamed x18 -> x10, local copies, waits for them, and re-layouts: 2.18 us -> 7.57 us
    convert_element_type x3 -> x0, other arithmetic: 4.96 us -> none  [the longest x1 4.21 us: body(): float_rows = tokens.astype(jnp.float32)]
  transfers between devices with their start and end apart: 6 -> 0, of which waited for: 5 -> 0; matrix products, arithmetic and copies ran while one was open for 6% -> 0% of each run, Pallas kernels for 0% -> 0%
where the time goes in v2:
time: 212 us
  Pallas kernels  203 us (96%)
  local copies, waits for them, and re-layouts  7.57 us (4%)
    pallas_call x1, Pallas kernels, body(): pl.pallas_call(kernel, out_shape=(weights, weights, weights, jax.ShapeDty...  203 us
    unnamed x10, local copies, waits for them, and re-layouts  7.57 us

profile of v2, /device:TPU:1, one launch (start us, length us, event | category | flops | bytes accessed | tf_op | source)
XLA Modules:
  0.0 211.5 jit_solution(14881076471146380466)
XLA Ops:
  0.6 203.3 %shard_map.102 = (bf16[32,64,512]{2,1,0:T(8,128)(2,1)}, bf16[32,64,512]{2,1,0:T(8,128)(2,1)}, bf16[32,64,512]{2,1,0:T(8,128)(2,1)}, bf16[512,256]{1,0:T(8,128)(2,1)}) custom-call(bf16[512,2048]{1,0:T(8,128)(2,1)} %tok_hbm.1, s32[2,512]{1,0:T(2,128)} %bitcast.9, f32[2,512]{1,0:T(2,128)} %bitcast.10, f32[1,64]{1,0:T(1,128)} %bitcast.11, ...), custom_call_target="tpu_custom_call" | custom-call | tf_op jit(solution)/shard_map/pallas_call | solution.py:335
  203.9 0.0 copy-start.1
  203.9 3.2 %copy.15 = bf16[1,2048,512]{2,1,0:T(8,128)(2,1)} copy(bf16[1,2048,512]{2,1,0:T(8,128)(2,1)} %bitcast.8) | data formatting | bytes 4194304
  207.1 0.0 copy-done.1
  207.1 0.0 copy-start
  207.1 1.3 copy.16
  208.5 1.0 copy-done
  209.5 0.0 copy-start.2
  209.5 1.3 copy.17
  210.8 0.0 copy-done.2
  210.8 0.7 copy.18
Async XLA Ops:
  203.9 3.2 %copy-start.1 = (bf16[32,64,512]{2,1,0:T(8,128)(2,1)S(1)}, bf16[32,64,512]{2,1,0:T(8,128)(2,1)}, u32[]{:S(2)}) copy-start(bf16[32,64,512]{2,1,0:T(8,128)(2,1)} %get-tuple-element.9) | copy-start | bytes 6291460
  207.1 2.3 %copy-start = (bf16[32,64,512]{2,1,0:T(8,128)(2,1)S(1)}, bf16[32,64,512]{2,1,0:T(8,128)(2,1)}, u32[]{:S(2)}) copy-start(bf16[32,64,512]{2,1,0:T(8,128)(2,1)} %get-tuple-element.10) | copy-start | bytes 6291460
  209.5 1.3 copy-start.2

commit v3 on v2

v3 whole, which is shorter than its diff:
```python
import functools

import jax
import jax.numpy as jnp
from jax import lax
from jax.experimental import pallas as pl
from jax.experimental.pallas import tpu as pltpu
from jax.sharding import PartitionSpec as P

MESH = pl.DeviceIdType.MESH
F32, BF16 = jnp.float32, jnp.bfloat16
EPSILON = 1e-05
D, UNITS, EXPERTS, TOK, CAP, TP, SOURCES = 2048, 512, 16, 512, 96, 8, 32
PART = D // TP
ROWS = EXPERTS * CAP
ROUNDS, DEPTH, LANES = 4, 16, 128
PACKED = ROWS // 2
EARLY = 12


def iota(shape, axis):
    return lax.broadcasted_iota(jnp.int32, shape, axis)


def kernel(
    tok_hbm, routes_hbm, weight_hbm, gain_hbm, wg_hbm, wu_hbm, wd_hbm,
    gate_in, up_in, down_in, mixed_ref,
    routes_ref, weight_ref, gain_ref, tok, mine, normed, dest, cmap, gate_own, up_own, outgoing, rows, hidden,
    pair_out, pair_in, own, chip, relay, merged, ring_in, result, back,
    load_sem, self_sem, gu_send, gu_recv, dn_send, dn_recv, tok_send, tok_recv,
    y_send, y_recv, core_send, core_recv, pair_send, pair_recv, ring_send, ring_recv, back_send, back_recv,
):
    gr, fs, tp = lax.axis_index("gr"), lax.axis_index("fs"), lax.axis_index("tp")
    z, x = gr * 4 + fs // 4, fs % 4
    y, core = tp // 2, tp % 2
    me = gr * 16 + fs
    odd = z % 2

    def plane(z2, x2):
        return {"gr": z2 // 4, "fs": (z2 % 4) * 4 + x2, "tp": tp}

    def peer(k):
        i, turn = k // 4, k % 4
        far = (i + 1) // 2
        step = (i % 2) * far + (1 - i % 2) * ((8 - far) % 8)
        turn = (i % 2) * turn + (1 - i % 2) * ((4 - turn) % 4)
        return (z + step) % 8, (x + turn) % 4

    def column(y2, core2):
        return {"gr": gr, "fs": fs, "tp": y2 * 2 + core2}

    def remote(src, dst, send, recv, device):
        return pltpu.make_async_remote_copy(
            src_ref=src, dst_ref=dst, send_sem=send, recv_sem=recv, device_id=device, device_id_type=MESH
        )

    def drained(ref, sem):
        pltpu.make_async_copy(ref, ref, sem).wait()

    barrier = pltpu.get_barrier_semaphore()

    def greet(k, carry):
        pl.semaphore_signal(barrier, inc=1, device_id=plane(*peer(32 - k)), device_id_type=MESH)
        return carry

    lax.fori_loop(1, 32, greet, 0)
    for turn in range(1, 4):
        pl.semaphore_signal(barrier, inc=1, device_id=column((y + turn) % 4, core), device_id_type=MESH)
    pl.semaphore_signal(barrier, inc=1, device_id=column(y, 1 - core), device_id_type=MESH)

    loads = [
        pltpu.make_async_copy(wg_hbm, gate_own, load_sem.at[0]),
        pltpu.make_async_copy(wu_hbm, up_own, load_sem.at[1]),
        pltpu.make_async_copy(tok_hbm, tok, load_sem.at[2]),
        pltpu.make_async_copy(tok_hbm.at[:, pl.ds(pl.multiple_of(tp * PART, PART), PART)], mine, load_sem.at[3]),
    ]
    loads += [
        pltpu.make_async_copy(src, dst, load_sem.at[4 + n])
        for n, (src, dst) in enumerate(((routes_hbm, routes_ref), (weight_hbm, weight_ref), (gain_hbm, gain_ref)))
    ]
    for load in loads:
        load.start()

    for load in loads[4:]:
        load.wait()
    diagonal = iota((64, 64), 0) == iota((64, 64), 1)
    gain = jnp.sum(jnp.where(diagonal, gain_ref[...], 0.0), axis=1, keepdims=True)
    loads[0].wait()
    loads[1].wait()

    def scale(e, carry):
        for ref in (gate_own, up_own):
            ref[e] = (ref[e].astype(F32) * gain).astype(BF16)
        return carry

    lax.fori_loop(0, EXPERTS, scale, 0)

    r0, r1 = routes_ref[0:1, :].astype(F32), routes_ref[1:2, :].astype(F32)
    names = iota((EXPERTS, TOK), 0).astype(F32)
    named = jnp.where((names == r0) | (names == r1), 1.0, 0.0)
    earlier = jnp.where(iota((TOK, TOK), 0) < iota((TOK, TOK), 1), 1.0, 0.0).astype(BF16)
    ranks = jnp.dot(named.astype(BF16), earlier, preferred_element_type=F32)
    for k, name in enumerate((r0, r1)):
        rank = jnp.sum(jnp.where(names == name, ranks, 0.0), axis=0, keepdims=True)
        dest[k : k + 1, :] = name * CAP + rank
        late = jnp.where(rank >= CAP // 2, float(PACKED - CAP // 2), 0.0)
        dest[2 + k : 3 + k, :] = name * (CAP // 2) + rank + late

    pl.semaphore_wait(barrier, 35)

    def send_gu(k, carry):
        z2, x2 = peer(k)
        e = (z2 % 4) * 4 + x2
        remote(gate_own.at[e], gate_in.at[me], gu_send.at[0], gu_recv.at[0], plane(z2, x2)).start()
        remote(up_own.at[e], up_in.at[me], gu_send.at[1], gu_recv.at[1], plane(z2, x2)).start()
        return carry

    lax.fori_loop(1, EARLY, send_gu, 0)

    loads[2].wait()
    loads[3].wait()

    def norm(b, carry):
        at = pl.ds(pl.multiple_of(b * 64, 64), 64)
        full = tok[at, :].astype(F32)
        inverse = lax.rsqrt(jnp.mean(full * full, axis=-1, keepdims=True) + EPSILON)
        normed[at, :] = (mine[at, :].astype(F32) * inverse).astype(BF16)
        return carry

    lax.fori_loop(0, TOK // 64, norm, 0)

    def pick(e, carry):
        slot = (iota((CAP, TOK), 0) + e * CAP).astype(F32)
        hits = jnp.where((slot == dest[0:1, :]) | (slot == dest[1:2, :]), 1.0, 0.0).astype(BF16)
        outgoing[e] = jnp.dot(hits, normed[...], preferred_element_type=F32).astype(BF16)
        return carry

    lax.fori_loop(0, EXPERTS, pick, 0)

    def slot_at(z2, z1):
        return (z1 - z2 + 2 - z2 % 2 + 16) % 8

    home = slot_at(z, z) * 4 + x

    def block(slot):
        return pl.ds(pl.multiple_of(slot * CAP, CAP), CAP)

    steps = [0, 1, 7, (1 - odd) * 2 + odd * 6]
    tok_self = pltpu.make_async_copy(outgoing.at[fs], rows.at[tp, block(home)], self_sem.at[0])
    tok_self.start()
    for i in range(4):
        for turn in range(4):
            if i + turn:
                z2, x2 = (z + steps[i]) % 8, (x + turn) % 4
                remote(
                    outgoing.at[(z2 % 4) * 4 + x2], rows.at[tp, block(slot_at(z2, z) * 4 + x)],
                    tok_send, tok_recv, plane(z2, x2),
                ).start()

    selves = [
        pltpu.make_async_copy(gate_own.at[fs], gate_in.at[me], self_sem.at[1]),
        pltpu.make_async_copy(up_own.at[fs], up_in.at[me], self_sem.at[2]),
        pltpu.make_async_copy(wd_hbm.at[fs], down_in.at[me], self_sem.at[3]),
    ]
    for copy in selves:
        copy.start()

    lax.fori_loop(EARLY, 32, send_gu, 0)

    def band(r):
        return pl.ds(pl.multiple_of(r * DEPTH, DEPTH), DEPTH)

    def send_dn(n, carry):
        r, k = n // 31, n % 31 + 1
        z2, x2 = peer(k)
        remote(
            wd_hbm.at[(z2 % 4) * 4 + x2, band(r)], down_in.at[me, band(r)],
            dn_send, dn_recv.at[r], plane(z2, x2),
        ).start()
        return carry

    lax.fori_loop(0, 31 * ROUNDS, send_dn, 0)

    across = iota((TOK, TOK), 0) == iota((TOK, TOK), 1)

    def upright(row):
        return jnp.sum(jnp.where(across, row, 0.0), axis=1, keepdims=True)

    mine_cols = jnp.concatenate(
        [upright(dest[2:3, :]), upright(dest[3:4, :]), upright(weight_ref[0:1, :]), upright(weight_ref[1:2, :])], axis=1
    )
    for b in range(8):
        cols = mine_cols[b * 64 : (b + 1) * 64]
        slot = iota((64, ROWS), 1).astype(F32)
        cmap[b * 64 : (b + 1) * 64, :] = (
            jnp.where(slot == cols[:, 0:1], cols[:, 2:3], 0.0) + jnp.where(slot == cols[:, 1:2], cols[:, 3:4], 0.0)
        ).astype(BF16)

    tok_self.wait()
    drained(outgoing.at[0:15], tok_recv)
    turns = (1, 3, 2)
    y_copies = [
        remote(rows.at[tp], rows.at[tp], y_send.at[turn - 1], y_recv.at[turn - 1], column((y + turn) % 4, core))
        for turn in turns
    ]
    for copy in y_copies:
        copy.start()
    core_copies = [remote(rows.at[tp], rows.at[tp], core_send.at[0], core_recv.at[0], column(y, 1 - core))]
    core_copies[0].start()
    for turn in turns:
        origin = ((y - turn + 4) % 4) * 2 + core
        drained(rows.at[origin], y_recv.at[turn - 1])
        core_copies.append(
            remote(rows.at[origin], rows.at[origin], core_send.at[turn], core_recv.at[turn], column(y, 1 - core))
        )
        core_copies[-1].start()
    for copy in core_copies:
        copy.wait_recv()

    for copy in selves:
        copy.wait()
    drained(gate_in.at[0:31], gu_recv.at[0])
    drained(up_in.at[0:31], gu_recv.at[1])

    def units(m, carry):
        at = pl.ds(pl.multiple_of(m * 4 * CAP, 4 * CAP), 4 * CAP)
        gate, upper = jnp.zeros((4 * CAP, UNITS), F32), jnp.zeros((4 * CAP, UNITS), F32)
        for j in range(TP):
            lhs = rows[j, at, :]
            gate += jnp.dot(lhs, gate_in[4 * j : 4 * j + 4].reshape(PART, UNITS), preferred_element_type=F32)
            upper += jnp.dot(lhs, up_in[4 * j : 4 * j + 4].reshape(PART, UNITS), preferred_element_type=F32)
        value = (gate / (1.0 + jnp.exp(-gate)) * upper).astype(BF16).reshape(4, 2, CAP // 2, UNITS)
        for half in range(2):
            hidden[half, pl.ds(4 * m, 4)] = value[:, half]
        return carry

    lax.fori_loop(0, EXPERTS // 4, units, 0)

    left = iota((8 * CAP // 2, LANES), 1) < LANES // 2
    pair_copies, ring_copies = [], []

    def half_block(slot):
        return pl.ds(pl.multiple_of(slot * (CAP // 2), CAP // 2), CAP // 2)

    def sum_cores(r):
        drained(down_in.at[0:31, 0:DEPTH], dn_recv.at[r])

        def partial(parity, store):
            down = jnp.concatenate(
                [
                    down_in[pl.ds(4 * (2 * k + parity), 4), r * DEPTH : (r + 1) * DEPTH].reshape(4 * DEPTH, UNITS)
                    for k in range(4)
                ],
                axis=0,
            )

            for m in range(2):
                outs = [
                    lax.dot_general(
                        hidden[half, 8 * m : 8 * m + 8].reshape(4 * CAP, UNITS), down, (((1,), (1,)), ((), ())),
                        preferred_element_type=F32,
                    )
                    for half in range(2)
                ]
                for two in range(2):
                    lanes = slice(two * LANES, (two + 1) * LANES)
                    low, high = outs[0][:, lanes], outs[1][:, lanes]
                    at = slice(m * 4 * CAP, (m + 1) * 4 * CAP)
                    store(2 * two, at, jnp.where(left, low, pltpu.roll(high, LANES // 2, 1)))
                    store(2 * two + 1, at, jnp.where(left, pltpu.roll(low, LANES // 2, 1), high))

        def give(y2, at, value):
            pair_out[r, y2, at, :] = value.astype(BF16)

        def keep(y2, at, value):
            own[r, y2, at, :] = value

        partial(1 - core, give)
        for turn in (2, 1, 3, 0):
            y2 = (y + turn) % 4
            pair_copies.append(
                remote(
                    pair_out.at[r, y2], pair_in.at[r, y2], pair_send.at[r, y2], pair_recv.at[r, y2],
                    column(y, 1 - core),
                )
            )
            pair_copies[-1].start()
        partial(core, keep)
        low, high = slice(0, PACKED // 2), slice(PACKED // 2, PACKED)
        sides = ((0, (y + 1) % 4, low, high), (1, (y + 3) % 4, high, low))

        def ring(n, src, dst, device):
            ring_copies.append(remote(src, dst, ring_send.at[r, n], ring_recv.at[r, n], device))
            ring_copies[-1].start()

        for n, turn in enumerate((2, 1, 3, 0)):
            y2 = (y + turn) % 4
            pair_copies[4 * r + n].wait_recv()
            chip[r, y2] = (own[r, y2] + pair_in[r, y2].astype(F32)).astype(BF16)
            if turn == 2:
                for n, near, first, _ in sides:
                    ring(n, chip.at[r, y2, first], relay.at[r, n], column(near, core))
        for n, near, _, second in sides:
            ring(2 + n, chip.at[r, near, second], ring_in.at[r, n, second], column(near, core))
        for n, near, first, _ in sides:
            ring_copies[6 * r + n].wait_recv()
            merged[r, n] = (chip[r, near, first].astype(F32) + relay[r, n].astype(F32)).astype(BF16)
            ring(4 + n, merged.at[r, n], ring_in.at[r, n, first], column(near, core))

    def sum_chips(r):
        for copy in ring_copies[6 * r + 2 : 6 * r + 6]:
            copy.wait_recv()
        value = chip[r, y].astype(F32)
        for n in range(2):
            value += ring_in[r, n].astype(F32)
        result[r] = value.astype(BF16)
        selves.append(pltpu.make_async_copy(result.at[r, half_block(home)], back.at[r, fs], self_sem.at[4 + r]))
        selves[-1].start()
        backs = [0, 1, 7, (1 - odd) * 6 + odd * 2]
        for i in (3, 1, 2, 0):
            for turn in range(4):
                if i + turn:
                    z1, x1 = (z + backs[i]) % 8, (x + turn) % 4
                    remote(
                        result.at[r, half_block(slot_at(z, z1) * 4 + x1)], back.at[r, fs],
                        back_send.at[r], back_recv.at[r], plane(z1, x1),
                    ).start()

    for r in range(ROUNDS):
        sum_cores(r)
        if r:
            sum_chips(r - 1)
    sum_chips(ROUNDS - 1)

    mixes = []
    for r in range(ROUNDS):
        selves[3 + r].wait()
        drained(back.at[r, 0:15], back_recv.at[r])
        returned = back[r].reshape(PACKED, LANES)
        low = jnp.dot(cmap[:, :PACKED], returned, preferred_element_type=F32)
        high = jnp.dot(cmap[:, PACKED:], returned, preferred_element_type=F32)
        mixes.append(low + pltpu.roll(high, LANES // 2, 1))
    first = iota((TOK, LANES), 1) < LANES // 2
    mixed = jnp.concatenate(
        [jnp.where(first, mixes[k], pltpu.roll(mixes[k + 1], LANES // 2, 1)) for k in (0, 2)], axis=1
    ).astype(BF16)
    a, b = iota((PART, PART), 0), iota((PART, PART), 1)
    order = jnp.where((a % 64) // DEPTH * 64 + a // 64 * DEPTH + a % DEPTH == b, 1.0, 0.0).astype(BF16)
    mixed_ref[...] = jnp.dot(mixed, order, preferred_element_type=F32).astype(BF16)

    drained(outgoing.at[0:15], tok_send)
    drained(gate_in.at[0:31], gu_send.at[0])
    drained(up_in.at[0:31], gu_send.at[1])
    drained(down_in.at[0:31], dn_send)
    for r in range(ROUNDS):
        drained(back.at[r, 0:15], back_send.at[r])
    for copy in y_copies + core_copies + pair_copies + ring_copies:
        copy.wait_send()


def body(tokens, routes, route_weight, gain, w_gate, w_up, w_down):
    anywhere = pl.BlockSpec(memory_space=pl.ANY)
    vmem = pl.BlockSpec(memory_space=pltpu.VMEM)
    weights = pltpu.VMEM((SOURCES, 64, UNITS), BF16)
    dma = pltpu.SemaphoreType.DMA
    gate_out, up_out, down_out, mixed = pl.pallas_call(
        kernel,
        out_shape=(weights, weights, weights, pltpu.VMEM((TOK, PART), BF16)),
        in_specs=[anywhere] * 7,
        out_specs=(vmem, vmem, vmem, vmem),
        scratch_shapes=[
            pltpu.VMEM((2, TOK), jnp.int32),
            pltpu.VMEM((2, TOK), F32),
            pltpu.VMEM((1, D // SOURCES), F32),
            pltpu.VMEM((TOK, D), BF16),
            pltpu.VMEM((TOK, PART), BF16),
            pltpu.VMEM((TOK, PART), BF16),
            pltpu.VMEM((4, TOK), F32),
            pltpu.VMEM((TOK, ROWS), BF16),
            pltpu.VMEM((EXPERTS, 64, UNITS), BF16),
            pltpu.VMEM((EXPERTS, 64, UNITS), BF16),
            pltpu.VMEM((EXPERTS, CAP, PART), BF16),
            pltpu.VMEM((TP, ROWS, PART), BF16),
            pltpu.VMEM((2, EXPERTS, CAP // 2, UNITS), BF16),
            pltpu.VMEM((ROUNDS, 4, PACKED, LANES), BF16),
            pltpu.VMEM((ROUNDS, 4, PACKED, LANES), BF16),
            pltpu.VMEM((ROUNDS, 4, PACKED, LANES), F32),
            pltpu.VMEM((ROUNDS, 4, PACKED, LANES), BF16),
            pltpu.VMEM((ROUNDS, 2, PACKED // 2, LANES), BF16),
            pltpu.VMEM((ROUNDS, 2, PACKED // 2, LANES), BF16),
            pltpu.VMEM((ROUNDS, 2, PACKED, LANES), BF16),
            pltpu.VMEM((ROUNDS, PACKED, LANES), BF16),
            pltpu.VMEM((ROUNDS, EXPERTS, CAP // 2, LANES), BF16),
            dma((7,)),
            dma((8,)),
            dma((2,)), dma((2,)),
            dma, dma((ROUNDS,)),
            dma, dma,
            dma((3,)), dma((3,)),
            dma((4,)), dma((4,)),
            dma((ROUNDS, 4)), dma((ROUNDS, 4)),
            dma((ROUNDS, 6)), dma((ROUNDS, 6)),
            dma((ROUNDS,)), dma((ROUNDS,)),
        ],
        compiler_params=pltpu.CompilerParams(
            collective_id=0, has_side_effects=True, vmem_limit_bytes=52 * 1024 * 1024
        ),
    )(tokens, routes.T, route_weight.T, gain.reshape(1, -1), w_gate, w_up, w_down)
    return tuple(w.reshape(1, D, UNITS) for w in (gate_out, up_out, down_out)) + (mixed,)


def solution(mesh):
    rows = ("gr", "fs")
    weights = P(None, rows, "tp")
    placed = P("fs", None, "tp")
    return jax.shard_map(
        body,
        mesh=mesh,
        in_specs=(P(rows, None), P(rows, None), P(rows, None), P(rows), weights, weights, weights),
        out_specs=(placed, placed, placed, P(rows, "tp")),
        check_vma=False,
    )
```

time: 212 us -> 188 us (0.89)
  Pallas kernels: 203 us -> 182 us
  local copies, waits for them, and re-layouts: 7.57 us -> 4.66 us
    pallas_call x1, Pallas kernels: 203 us -> 182 us  [body(): pl.pallas_call(kernel, out_shape=(weights, weights, weights, pltpu.VMEM((...]
    unnamed x10 -> x4, local copies, waits for them, and re-layouts: 7.57 us -> 4.66 us
where the time goes in v3:
time: 188 us
  Pallas kernels  182 us (97%)
  local copies, waits for them, and re-layouts  4.66 us (2%)
    pallas_call x1, Pallas kernels, body(): pl.pallas_call(kernel, out_shape=(weights, weights, weights, pltpu.VMEM((...  182 us
    unnamed x4, local copies, waits for them, and re-layouts  4.66 us

profile of v3, /device:TPU:1, one launch (start us, length us, event | category | flops | bytes accessed | tf_op | source)
XLA Modules:
  0.0 187.7 jit_solution(14172066945962112852)
XLA Ops:
  0.6 182.4 %shard_map.102 = (bf16[32,64,512]{2,1,0:T(8,128)(2,1)S(1)}, bf16[32,64,512]{2,1,0:T(8,128)(2,1)S(1)}, bf16[32,64,512]{2,1,0:T(8,128)(2,1)S(1)}, bf16[512,256]{1,0:T(8,128)(2,1)S(1)}) custom-call(bf16[512,2048]{1,0:T(8,128)(2,1)} %tok_hbm.1, s32[2,512]{1,0:T(2,128)} %bitcast.9, f32[2,512]{1,0:T(2,128)} %bitcast.10, f32[1,64]{1,0:T(1,128)} %bitcast.11, ...), custom_call_target="tpu_custom_call" | custom-call | tf_op jit(solution)/shard_map/pallas_call | solution.py:366
  183.0 1.3 copy.15
  184.3 1.3 copy.16
  185.6 0.7 copy.18
  186.3 1.3 copy.17

commit v4 on v3

--- a/solution.py
+++ b/solution.py
@@ -22,10 +22,39 @@
     return lax.broadcasted_iota(jnp.int32, shape, axis)
 
 
+def mix_of(cmap, returned):
+    returned = returned.reshape(PACKED, LANES)
+    low = jnp.dot(cmap[:, :PACKED], returned, preferred_element_type=F32)
+    high = jnp.dot(cmap[:, PACKED:], returned, preferred_element_type=F32)
+    return low + pltpu.roll(high, LANES // 2, 1)
+
+
+def in_lanes(one, other):
+    first = iota((TOK, LANES), 1) < LANES // 2
+    return jnp.where(first, one, pltpu.roll(other, LANES // 2, 1))
+
+
+def finish(gate_in, up_in, down_in, cmap, begun_ref, back_ref, gate_hbm, up_hbm, down_hbm, mixed_hbm, mixed, sem):
+    copies = [
+        pltpu.make_async_copy(src, dst, sem.at[n])
+        for n, (src, dst) in enumerate(((gate_in, gate_hbm), (up_in, up_hbm), (down_in, down_hbm), (mixed, mixed_hbm)))
+    ]
+    for copy in copies[:3]:
+        copy.start()
+    ended = in_lanes(begun_ref[:, LANES:], mix_of(cmap, back_ref[...]))
+    values = jnp.concatenate([begun_ref[:, :LANES], ended], axis=1).astype(BF16)
+    a, b = iota((PART, PART), 0), iota((PART, PART), 1)
+    order = jnp.where((a % 64) // DEPTH * 64 + a // 64 * DEPTH + a % DEPTH == b, 1.0, 0.0).astype(BF16)
+    mixed[...] = jnp.dot(values, order, preferred_element_type=F32).astype(BF16)
+    copies[3].start()
+    for copy in copies:
+        copy.wait()
+
+
 def kernel(
     tok_hbm, routes_hbm, weight_hbm, gain_hbm, wg_hbm, wu_hbm, wd_hbm,
-    gate_in, up_in, down_in, mixed_ref,
-    routes_ref, weight_ref, gain_ref, tok, mine, normed, dest, cmap, gate_own, up_own, outgoing, rows, hidden,
+    gate_in, up_in, down_in, cmap, begun_ref, back_ref,
+    routes_ref, weight_ref, gain_ref, tok, mine, normed, dest, gate_own, up_own, outgoing, rows, hidden,
     pair_out, pair_in, own, chip, relay, merged, ring_in, result, back,
     load_sem, self_sem, gu_send, gu_recv, dn_send, dn_recv, tok_send, tok_recv,
     y_send, y_recv, core_send, core_recv, pair_send, pair_recv, ring_send, ring_recv, back_send, back_recv,
@@ -59,30 +88,38 @@
 
     barrier = pltpu.get_barrier_semaphore()
 
-    def greet(k, carry):
-        pl.semaphore_signal(barrier, inc=1, device_id=plane(*peer(32 - k)), device_id_type=MESH)
-        return carry
-
-    lax.fori_loop(1, 32, greet, 0)
-    for turn in range(1, 4):
-        pl.semaphore_signal(barrier, inc=1, device_id=column((y + turn) % 4, core), device_id_type=MESH)
-    pl.semaphore_signal(barrier, inc=1, device_id=column(y, 1 - core), device_id_type=MESH)
+    def greet(device):
+        pl.semaphore_signal(barrier, inc=1, device_id=device, device_id_type=MESH)
+
+    turns_x = [(x + turn) % 4 for turn in range(4)]
+    for step in (4, 3, 5, 2, 6, 1, 7, 0):
+        z2 = (z + step) % 8
+        half, first = z2 // 4, z2 % 4 * 4
+        for turn in (2, 1, 3, 0):
+            if step + turn:
+                greet({"gr": half, "fs": first + turns_x[turn], "tp": tp})
+    for turn in (2, 1, 3):
+        greet(column((y + turn) % 4, core))
+    greet(column(y, 1 - core))
 
     loads = [
-        pltpu.make_async_copy(wg_hbm, gate_own, load_sem.at[0]),
-        pltpu.make_async_copy(wu_hbm, up_own, load_sem.at[1]),
-        pltpu.make_async_copy(tok_hbm, tok, load_sem.at[2]),
-        pltpu.make_async_copy(tok_hbm.at[:, pl.ds(pl.multiple_of(tp * PART, PART), PART)], mine, load_sem.at[3]),
+        pltpu.make_async_copy(src, dst, load_sem.at[n])
+        for n, (src, dst) in enumerate(
+            (
+                (wg_hbm, gate_own),
+                (wu_hbm, up_own),
+                (tok_hbm, tok),
+                (tok_hbm.at[:, pl.ds(pl.multiple_of(tp * PART, PART), PART)], mine),
+                (routes_hbm, routes_ref),
+                (weight_hbm, weight_ref),
+                (gain_hbm, gain_ref),
+            )
+        )
     ]
-    loads += [
-        pltpu.make_async_copy(src, dst, load_sem.at[4 + n])
-        for n, (src, dst) in enumerate(((routes_hbm, routes_ref), (weight_hbm, weight_ref), (gain_hbm, gain_ref)))
-    ]
-    for load in loads:
+    for load in (loads[6], *loads[:6]):
         load.start()
 
-    for load in loads[4:]:
-        load.wait()
+    loads[6].wait()
     diagonal = iota((64, 64), 0) == iota((64, 64), 1)
     gain = jnp.sum(jnp.where(diagonal, gain_ref[...], 0.0), axis=1, keepdims=True)
     loads[0].wait()
@@ -95,6 +132,8 @@
 
     lax.fori_loop(0, EXPERTS, scale, 0)
 
+    loads[4].wait()
+    loads[5].wait()
     r0, r1 = routes_ref[0:1, :].astype(F32), routes_ref[1:2, :].astype(F32)
     names = iota((EXPERTS, TOK), 0).astype(F32)
     named = jnp.where((names == r0) | (names == r1), 1.0, 0.0)
@@ -242,6 +281,19 @@
     def half_block(slot):
         return pl.ds(pl.multiple_of(slot * (CAP // 2), CAP // 2), CAP // 2)
 
+    def give_back(r):
+        selves.append(pltpu.make_async_copy(result.at[r, half_block(home)], back.at[r, fs], self_sem.at[4 + r]))
+        selves[-1].start()
+        backs = [0, 1, 7, (1 - odd) * 6 + odd * 2]
+        for i in (3, 1, 2, 0):
+            for turn in range(4):
+                if i + turn:
+                    z1, x1 = (z + backs[i]) % 8, (x + turn) % 4
+                    remote(
+                        result.at[r, half_block(slot_at(z, z1) * 4 + x1)], back.at[r, fs],
+                        back_send.at[r], back_recv.at[r], plane(z1, x1),
+                    ).start()
+
     def sum_cores(r):
         drained(down_in.at[0:31, 0:DEPTH], dn_recv.at[r])
 
@@ -302,6 +354,9 @@
                     ring(n, chip.at[r, y2, first], relay.at[r, n], column(near, core))
         for n, near, _, second in sides:
             ring(2 + n, chip.at[r, near, second], ring_in.at[r, n, second], column(near, core))
+        if r == ROUNDS - 1:
+            for before in range(r - 1):
+                give_back(before)
         for n, near, first, _ in sides:
             ring_copies[6 * r + n].wait_recv()
             merged[r, n] = (chip[r, near, first].astype(F32) + relay[r, n].astype(F32)).astype(BF16)
@@ -314,39 +369,24 @@
         for n in range(2):
             value += ring_in[r, n].astype(F32)
         result[r] = value.astype(BF16)
-        selves.append(pltpu.make_async_copy(result.at[r, half_block(home)], back.at[r, fs], self_sem.at[4 + r]))
-        selves[-1].start()
-        backs = [0, 1, 7, (1 - odd) * 6 + odd * 2]
-        for i in (3, 1, 2, 0):
-            for turn in range(4):
-                if i + turn:
-                    z1, x1 = (z + backs[i]) % 8, (x + turn) % 4
-                    remote(
-                        result.at[r, half_block(slot_at(z, z1) * 4 + x1)], back.at[r, fs],
-                        back_send.at[r], back_recv.at[r], plane(z1, x1),
-                    ).start()
-
-    for r in range(ROUNDS):
-        sum_cores(r)
-        if r:
-            sum_chips(r - 1)
-    sum_chips(ROUNDS - 1)
-
-    mixes = []
-    for r in range(ROUNDS):
+
+    def mix(r):
         selves[3 + r].wait()
         drained(back.at[r, 0:15], back_recv.at[r])
-        returned = back[r].reshape(PACKED, LANES)
-        low = jnp.dot(cmap[:, :PACKED], returned, preferred_element_type=F32)
-        high = jnp.dot(cmap[:, PACKED:], returned, preferred_element_type=F32)
-        mixes.append(low + pltpu.roll(high, LANES // 2, 1))
-    first = iota((TOK, LANES), 1) < LANES // 2
-    mixed = jnp.concatenate(
-        [jnp.where(first, mixes[k], pltpu.roll(mixes[k + 1], LANES // 2, 1)) for k in (0, 2)], axis=1
-    ).astype(BF16)
-    a, b = iota((PART, PART), 0), iota((PART, PART), 1)
-    order = jnp.where((a % 64) // DEPTH * 64 + a // 64 * DEPTH + a % DEPTH == b, 1.0, 0.0).astype(BF16)
-    mixed_ref[...] = jnp.dot(mixed, order, preferred_element_type=F32).astype(BF16)
+        return mix_of(cmap, back[r])
+
+    sum_cores(0)
+    for r in range(1, ROUNDS):
+        sum_cores(r)
+        sum_chips(r - 1)
+    give_back(ROUNDS - 2)
+    sum_chips(ROUNDS - 1)
+    give_back(ROUNDS - 1)
+    begun_ref[:, :LANES] = in_lanes(mix(0), mix(1))
+    begun_ref[:, LANES:] = mix(2)
+    selves[6].wait()
+    drained(back.at[3, 0:15], back_recv.at[3])
+    back_ref[...] = back[3]
 
     drained(outgoing.at[0:15], tok_send)
     drained(gate_in.at[0:31], gu_send.at[0])
@@ -363,11 +403,16 @@
     vmem = pl.BlockSpec(memory_space=pltpu.VMEM)
     weights = pltpu.VMEM((SOURCES, 64, UNITS), BF16)
     dma = pltpu.SemaphoreType.DMA
-    gate_out, up_out, down_out, mixed = pl.pallas_call(
+    held = pl.pallas_call(
         kernel,
-        out_shape=(weights, weights, weights, pltpu.VMEM((TOK, PART), BF16)),
+        out_shape=(
+            weights, weights, weights,
+            pltpu.VMEM((TOK, ROWS), BF16),
+            pltpu.VMEM((TOK, 2 * LANES), F32),
+            pltpu.VMEM((EXPERTS, CAP // 2, LANES), BF16),
+        ),
         in_specs=[anywhere] * 7,
-        out_specs=(vmem, vmem, vmem, vmem),
+        out_specs=(vmem,) * 6,
         scratch_shapes=[
             pltpu.VMEM((2, TOK), jnp.int32),
             pltpu.VMEM((2, TOK), F32),
@@ -376,7 +421,6 @@
             pltpu.VMEM((TOK, PART), BF16),
             pltpu.VMEM((TOK, PART), BF16),
             pltpu.VMEM((4, TOK), F32),
-            pltpu.VMEM((TOK, ROWS), BF16),
             pltpu.VMEM((EXPERTS, 64, UNITS), BF16),
             pltpu.VMEM((EXPERTS, 64, UNITS), BF16),
             pltpu.VMEM((EXPERTS, CAP, PART), BF16),
@@ -403,9 +447,18 @@
             dma((ROUNDS,)), dma((ROUNDS,)),
         ],
         compiler_params=pltpu.CompilerParams(
-            collective_id=0, has_side_effects=True, vmem_limit_bytes=52 * 1024 * 1024
+            collective_id=0, has_side_effects=True, vmem_limit_bytes=48 * 1024 * 1024
         ),
     )(tokens, routes.T, route_weight.T, gain.reshape(1, -1), w_gate, w_up, w_down)
+    placed = jax.ShapeDtypeStruct((SOURCES, 64, UNITS), BF16)
+    gate_out, up_out, down_out, mixed = pl.pallas_call(
+        finish,
+        out_shape=(placed, placed, placed, jax.ShapeDtypeStruct((TOK, PART), BF16)),
+        in_specs=[vmem] * 6,
+        out_specs=(anywhere,) * 4,
+        scratch_shapes=[pltpu.VMEM((TOK, PART), BF16), dma((4,))],
+        compiler_params=pltpu.CompilerParams(vmem_limit_bytes=16 * 1024 * 1024),
+    )(*held)
     return tuple(w.reshape(1, D, UNITS) for w in (gate_out, up_out, down_out)) + (mixed,)
 
 

time: 188 us -> 183 us (0.973)
  local copies, waits for them, and re-layouts: 4.66 us -> 0 us
    unnamed x4 -> x0, local copies, waits for them, and re-layouts: 4.66 us -> none
    pallas_call x0 -> x1, Pallas kernels: none -> 2.75 us  [body(): pl.pallas_call(finish, out_shape=(placed, placed, placed, jax.ShapeDtypeS...]
    pallas_call x1, Pallas kernels: 182 us -> 180 us  [body(): pl.pallas_call(kernel, out_shape=(weights, weights, weights, pltpu.VMEM((...]
where the time goes in v4:
time: 183 us
  Pallas kernels  183 us (100%)
    pallas_call x1, Pallas kernels, body(): pl.pallas_call(kernel, out_shape=(weights, weights, weights, pltpu.VMEM((...  180 us

profile of v4, /device:TPU:1, one launch (start us, length us, event | category | flops | bytes accessed | tf_op | source)
XLA Modules:
  0.0 183.2 jit_solution(15521436432425164696)
XLA Ops:
  0.6 179.8 %shard_map.102 = (bf16[32,64,512]{2,1,0:T(8,128)(2,1)S(1)}, bf16[32,64,512]{2,1,0:T(8,128)(2,1)S(1)}, bf16[32,64,512]{2,1,0:T(8,128)(2,1)S(1)}, bf16[512,1536]{1...) custom-call(bf16[512,2048]{1,0:T(8,128)(2,1)} %tok_hbm.1, s32[2,512]{1,0:T(2,128)} %bitcast.6, ...), custom_call_target="tpu_custom_call" | custom-call | tf_op jit(solution)/shard_map/pallas_call | solution.py:406
  180.5 2.8 %shard_map.103 = (bf16[32,64,512]{2,1,0:T(8,128)(2,1)}, bf16[32,64,512]{2,1,0:T(8,128)(2,1)}, bf16[32,64,512]{2,1,0:T(8,128)(2,1)}, bf16[512,256]{1,0:T(8,128)(2,1)}) custom-call(bf16[32,64,512]{2,1,0:T(8,128)(2,1)S(1)} %get-tuple-element.14.gate_in, bf16[32,64,512]{2,1,0:T(8,128)(2,1)S(1)} %get-tuple-element.15.up_in, ...), custom_call_target="tpu_custom_call" | custom-call | tf_op jit(solution)/shard_map/pallas_call | solution.py:454

commit v5 on v4

--- a/solution.py
+++ b/solution.py
@@ -54,7 +54,7 @@
 def kernel(
     tok_hbm, routes_hbm, weight_hbm, gain_hbm, wg_hbm, wu_hbm, wd_hbm,
     gate_in, up_in, down_in, cmap, begun_ref, back_ref,
-    routes_ref, weight_ref, gain_ref, tok, mine, normed, dest, gate_own, up_own, outgoing, rows, hidden,
+    routes_ref, weight_ref, gain_ref, tok, mine, normed, dest, gate_own, up_own, down_own, outgoing, rows, hidden,
     pair_out, pair_in, own, chip, relay, merged, ring_in, result, back,
     load_sem, self_sem, gu_send, gu_recv, dn_send, dn_recv, tok_send, tok_recv,
     y_send, y_recv, core_send, core_recv, pair_send, pair_recv, ring_send, ring_recv, back_send, back_recv,
@@ -113,10 +113,11 @@
                 (routes_hbm, routes_ref),
                 (weight_hbm, weight_ref),
                 (gain_hbm, gain_ref),
+                (wd_hbm, down_own),
             )
         )
     ]
-    for load in (loads[6], *loads[:6]):
+    for load in (loads[6], *loads[:6], loads[7]):
         load.start()
 
     loads[6].wait()
@@ -196,24 +197,25 @@
                     tok_send, tok_recv, plane(z2, x2),
                 ).start()
 
+    loads[7].wait()
     selves = [
         pltpu.make_async_copy(gate_own.at[fs], gate_in.at[me], self_sem.at[1]),
         pltpu.make_async_copy(up_own.at[fs], up_in.at[me], self_sem.at[2]),
-        pltpu.make_async_copy(wd_hbm.at[fs], down_in.at[me], self_sem.at[3]),
+        pltpu.make_async_copy(down_own.at[fs], down_in.at[me], self_sem.at[3]),
     ]
     for copy in selves:
         copy.start()
 
-    lax.fori_loop(EARLY, 32, send_gu, 0)
+    lax.fori_loop(EARLY, 32, lambda k, carry: send_gu(31 + EARLY - k, carry), 0)
 
     def band(r):
         return pl.ds(pl.multiple_of(r * DEPTH, DEPTH), DEPTH)
 
     def send_dn(n, carry):
-        r, k = n // 31, n % 31 + 1
+        r, k = n // 31, 31 - n % 31
         z2, x2 = peer(k)
         remote(
-            wd_hbm.at[(z2 % 4) * 4 + x2, band(r)], down_in.at[me, band(r)],
+            down_own.at[(z2 % 4) * 4 + x2, band(r)], down_in.at[me, band(r)],
             dn_send, dn_recv.at[r], plane(z2, x2),
         ).start()
         return carry
@@ -423,6 +425,7 @@
             pltpu.VMEM((4, TOK), F32),
             pltpu.VMEM((EXPERTS, 64, UNITS), BF16),
             pltpu.VMEM((EXPERTS, 64, UNITS), BF16),
+            pltpu.VMEM((EXPERTS, 64, UNITS), BF16),
             pltpu.VMEM((EXPERTS, CAP, PART), BF16),
             pltpu.VMEM((TP, ROWS, PART), BF16),
             pltpu.VMEM((2, EXPERTS, CAP // 2, UNITS), BF16),
@@ -435,7 +438,7 @@
             pltpu.VMEM((ROUNDS, 2, PACKED, LANES), BF16),
             pltpu.VMEM((ROUNDS, PACKED, LANES), BF16),
             pltpu.VMEM((ROUNDS, EXPERTS, CAP // 2, LANES), BF16),
-            dma((7,)),
+            dma((8,)),
             dma((8,)),
             dma((2,)), dma((2,)),
             dma, dma((ROUNDS,)),

time: 183 us -> 182 us (level)
  Pallas kernels: 183 us -> 181 us
where the time goes in v5:
time: 182 us
  Pallas kernels  181 us (99%)
    pallas_call x1, Pallas kernels, body(): pl.pallas_call(kernel, out_shape=(weights, weights, weights, pltpu.VMEM((...  178 us

profile of v5, /device:TPU:1, one launch (start us, length us, event | category | flops | bytes accessed | tf_op | source)
XLA Modules:
  0.0 181.7 jit_solution(5749905814925924674)
XLA Ops:
  0.6 178.3 %shard_map.102 = (bf16[32,64,512]{2,1,0:T(8,128)(2,1)S(1)}, bf16[32,64,512]{2,1,0:T(8,128)(2,1)S(1)}, bf16[32,64,512]{2,1,0:T(8,128)(2,1)S(1)}, bf16[512,1536]{1...) custom-call(bf16[512,2048]{1,0:T(8,128)(2,1)} %tok_hbm.1, s32[2,512]{1,0:T(2,128)} %bitcast.6, ...), custom_call_target="tpu_custom_call" | custom-call | tf_op jit(solution)/shard_map/pallas_call | solution.py:408
  178.9 2.8 %shard_map.103 = (bf16[32,64,512]{2,1,0:T(8,128)(2,1)}, bf16[32,64,512]{2,1,0:T(8,128)(2,1)}, bf16[32,64,512]{2,1,0:T(8,128)(2,1)}, bf16[512,256]{1,0:T(8,128)(2,1)}) custom-call(bf16[32,64,512]{2,1,0:T(8,128)(2,1)S(1)} %get-tuple-element.14.gate_in, bf16[32,64,512]{2,1,0:T(8,128)(2,1)S(1)} %get-tuple-element.15.up_in, ...), custom_call_target="tpu_custom_call" | custom-call | tf_op jit(solution)/shard_map/pallas_call | solution.py:457

commit v6 on v5

--- a/solution.py
+++ b/solution.py
@@ -56,7 +56,7 @@
     gate_in, up_in, down_in, cmap, begun_ref, back_ref,
     routes_ref, weight_ref, gain_ref, tok, mine, normed, dest, gate_own, up_own, down_own, outgoing, rows, hidden,
     pair_out, pair_in, own, chip, relay, merged, ring_in, result, back,
-    load_sem, self_sem, gu_send, gu_recv, dn_send, dn_recv, tok_send, tok_recv,
+    load_sem, wave_sem, self_sem, gu_send, gu_recv, dn_send, dn_recv, tok_send, tok_recv,
     y_send, y_recv, core_send, core_recv, pair_send, pair_recv, ring_send, ring_recv, back_send, back_recv,
 ):
     gr, fs, tp = lax.axis_index("gr"), lax.axis_index("fs"), lax.axis_index("tp")
@@ -92,7 +92,7 @@
         pl.semaphore_signal(barrier, inc=1, device_id=device, device_id_type=MESH)
 
     turns_x = [(x + turn) % 4 for turn in range(4)]
-    for step in (4, 3, 5, 2, 6, 1, 7, 0):
+    for step in (1, 7, 0):
         z2 = (z + step) % 8
         half, first = z2 // 4, z2 % 4 * 4
         for turn in (2, 1, 3, 0):
@@ -133,6 +133,29 @@
 
     lax.fori_loop(0, EXPERTS, scale, 0)
 
+    pl.semaphore_wait(barrier, 15)
+
+    def send_gu(k, carry):
+        z2, x2 = peer(k)
+        e = (z2 % 4) * 4 + x2
+        remote(gate_own.at[e], gate_in.at[me], gu_send.at[0], gu_recv.at[0], plane(z2, x2)).start()
+        remote(up_own.at[e], up_in.at[me], gu_send.at[1], gu_recv.at[1], plane(z2, x2)).start()
+        return carry
+
+    lax.fori_loop(1, EARLY, send_gu, 0)
+
+    def hail(n):
+        for side, step in ((0, 1), (1, 7)):
+            pl.semaphore_signal(
+                wave_sem.at[n, side], inc=1, device_id=plane((z + step) % 8, x), device_id_type=MESH
+            )
+
+    def heard(n):
+        for side in range(2):
+            pl.semaphore_wait(wave_sem.at[n, side], 1)
+
+    hail(0)
+
     loads[4].wait()
     loads[5].wait()
     r0, r1 = routes_ref[0:1, :].astype(F32), routes_ref[1:2, :].astype(F32)
@@ -146,17 +169,6 @@
         late = jnp.where(rank >= CAP // 2, float(PACKED - CAP // 2), 0.0)
         dest[2 + k : 3 + k, :] = name * (CAP // 2) + rank + late
 
-    pl.semaphore_wait(barrier, 35)
-
-    def send_gu(k, carry):
-        z2, x2 = peer(k)
-        e = (z2 % 4) * 4 + x2
-        remote(gate_own.at[e], gate_in.at[me], gu_send.at[0], gu_recv.at[0], plane(z2, x2)).start()
-        remote(up_own.at[e], up_in.at[me], gu_send.at[1], gu_recv.at[1], plane(z2, x2)).start()
-        return carry
-
-    lax.fori_loop(1, EARLY, send_gu, 0)
-
     loads[2].wait()
     loads[3].wait()
 
@@ -168,6 +180,8 @@
         return carry
 
     lax.fori_loop(0, TOK // 64, norm, 0)
+    heard(0)
+    hail(1)
 
     def pick(e, carry):
         slot = (iota((CAP, TOK), 0) + e * CAP).astype(F32)
@@ -176,6 +190,8 @@
         return carry
 
     lax.fori_loop(0, EXPERTS, pick, 0)
+    heard(1)
+    hail(2)
 
     def slot_at(z2, z1):
         return (z1 - z2 + 2 - z2 % 2 + 16) % 8
@@ -206,6 +222,7 @@
     for copy in selves:
         copy.start()
 
+    heard(2)
     lax.fori_loop(EARLY, 32, lambda k, carry: send_gu(31 + EARLY - k, carry), 0)
 
     def band(r):
@@ -439,6 +456,7 @@
             pltpu.VMEM((ROUNDS, PACKED, LANES), BF16),
             pltpu.VMEM((ROUNDS, EXPERTS, CAP // 2, LANES), BF16),
             dma((8,)),
+            pltpu.SemaphoreType.REGULAR((3, 2)),
             dma((8,)),
             dma((2,)), dma((2,)),
             dma, dma((ROUNDS,)),

time: 182 us -> 180 us (0.989)
  Pallas kernels: 181 us -> 179 us
where the time goes in v6:
time: 180 us
  Pallas kernels  179 us (99%)
    pallas_call x1, Pallas kernels, body(): pl.pallas_call(kernel, out_shape=(weights, weights, weights, pltpu.VMEM((...  177 us

profile of v6, /device:TPU:1, one launch (start us, length us, event | category | flops | bytes accessed | tf_op | source)
XLA Modules:
  0.0 180.0 jit_solution(4797738568969256267)
XLA Ops:
  0.6 176.6 %shard_map.102 = (bf16[32,64,512]{2,1,0:T(8,128)(2,1)S(1)}, bf16[32,64,512]{2,1,0:T(8,128)(2,1)S(1)}, bf16[32,64,512]{2,1,0:T(8,128)(2,1)S(1)}, bf16[512,1536]{1...) custom-call(bf16[512,2048]{1,0:T(8,128)(2,1)} %tok_hbm.1, s32[2,512]{1,0:T(2,128)} %bitcast.6, ...), custom_call_target="tpu_custom_call" | custom-call | tf_op jit(solution)/shard_map/pallas_call | solution.py:425
  177.2 2.8 %shard_map.103 = (bf16[32,64,512]{2,1,0:T(8,128)(2,1)}, bf16[32,64,512]{2,1,0:T(8,128)(2,1)}, bf16[32,64,512]{2,1,0:T(8,128)(2,1)}, bf16[512,256]{1,0:T(8,128)(2,1)}) custom-call(bf16[32,64,512]{2,1,0:T(8,128)(2,1)S(1)} %get-tuple-element.14.gate_in, bf16[32,64,512]{2,1,0:T(8,128)(2,1)S(1)} %get-tuple-element.15.up_in, ...), custom_call_target="tpu_custom_call" | custom-call | tf_op jit(solution)/shard_map/pallas_call | solution.py:475

commit v7 on v6

--- a/solution.py
+++ b/solution.py
@@ -142,7 +142,8 @@
         remote(up_own.at[e], up_in.at[me], gu_send.at[1], gu_recv.at[1], plane(z2, x2)).start()
         return carry
 
-    lax.fori_loop(1, EARLY, send_gu, 0)
+    lax.fori_loop(4, EARLY, send_gu, 0)
+    lax.fori_loop(1, 4, send_gu, 0)
 
     def hail(n):
         for side, step in ((0, 1), (1, 7)):
@@ -300,16 +301,19 @@
     def half_block(slot):
         return pl.ds(pl.multiple_of(slot * (CAP // 2), CAP // 2), CAP // 2)
 
+    backs = [back.at[r] for r in range(ROUNDS - 1)] + [back_ref]
+
     def give_back(r):
-        selves.append(pltpu.make_async_copy(result.at[r, half_block(home)], back.at[r, fs], self_sem.at[4 + r]))
+        home_back = backs[r].at[fs]
+        selves.append(pltpu.make_async_copy(result.at[r, half_block(home)], home_back, self_sem.at[4 + r]))
         selves[-1].start()
-        backs = [0, 1, 7, (1 - odd) * 6 + odd * 2]
+        homes = [0, 1, 7, (1 - odd) * 6 + odd * 2]
         for i in (3, 1, 2, 0):
             for turn in range(4):
                 if i + turn:
-                    z1, x1 = (z + backs[i]) % 8, (x + turn) % 4
+                    z1, x1 = (z + homes[i]) % 8, (x + turn) % 4
                     remote(
-                        result.at[r, half_block(slot_at(z, z1) * 4 + x1)], back.at[r, fs],
+                        result.at[r, half_block(slot_at(z, z1) * 4 + x1)], home_back,
                         back_send.at[r], back_recv.at[r], plane(z1, x1),
                     ).start()
 
@@ -404,15 +408,14 @@
     begun_ref[:, :LANES] = in_lanes(mix(0), mix(1))
     begun_ref[:, LANES:] = mix(2)
     selves[6].wait()
-    drained(back.at[3, 0:15], back_recv.at[3])
-    back_ref[...] = back[3]
+    drained(back_ref.at[0:15], back_recv.at[3])
 
     drained(outgoing.at[0:15], tok_send)
     drained(gate_in.at[0:31], gu_send.at[0])
     drained(up_in.at[0:31], gu_send.at[1])
     drained(down_in.at[0:31], dn_send)
     for r in range(ROUNDS):
-        drained(back.at[r, 0:15], back_send.at[r])
+        drained(backs[r].at[0:15], back_send.at[r])
     for copy in y_copies + core_copies + pair_copies + ring_copies:
         copy.wait_send()
 
@@ -454,7 +457,7 @@
             pltpu.VMEM((ROUNDS, 2, PACKED // 2, LANES), BF16),
             pltpu.VMEM((ROUNDS, 2, PACKED, LANES), BF16),
             pltpu.VMEM((ROUNDS, PACKED, LANES), BF16),
-            pltpu.VMEM((ROUNDS, EXPERTS, CAP // 2, LANES), BF16),
+            pltpu.VMEM((ROUNDS - 1, EXPERTS, CAP // 2, LANES), BF16),
             dma((8,)),
             pltpu.SemaphoreType.REGULAR((3, 2)),
             dma((8,)),

time: 180 us -> 180 us (level)
  no operation moved by 1% of the time
where the time goes in v7:
time: 180 us
  Pallas kernels  179 us (99%)
    pallas_call x1, Pallas kernels, body(): pl.pallas_call(kernel, out_shape=(weights, weights, weights, pltpu.VMEM((...  176 us

profile of v7, /device:TPU:1, one launch (start us, length us, event | category | flops | bytes accessed | tf_op | source)
XLA Modules:
  0.0 179.8 jit_solution(1911358644539780807)
XLA Ops:
  0.6 176.5 %shard_map.102 = (bf16[32,64,512]{2,1,0:T(8,128)(2,1)S(1)}, bf16[32,64,512]{2,1,0:T(8,128)(2,1)S(1)}, bf16[32,64,512]{2,1,0:T(8,128)(2,1)S(1)}, bf16[512,1536]{1...) custom-call(bf16[512,2048]{1,0:T(8,128)(2,1)} %tok_hbm.1, s32[2,512]{1,0:T(2,128)} %bitcast.6, ...), custom_call_target="tpu_custom_call" | custom-call | tf_op jit(solution)/shard_map/pallas_call | solution.py:428
  177.1 2.8 %shard_map.103 = (bf16[32,64,512]{2,1,0:T(8,128)(2,1)}, bf16[32,64,512]{2,1,0:T(8,128)(2,1)}, bf16[32,64,512]{2,1,0:T(8,128)(2,1)}, bf16[512,256]{1,0:T(8,128)(2,1)}) custom-call(bf16[32,64,512]{2,1,0:T(8,128)(2,1)S(1)} %get-tuple-element.14.gate_in, bf16[32,64,512]{2,1,0:T(8,128)(2,1)S(1)} %get-tuple-element.15.up_in, ...), custom_call_target="tpu_custom_call" | custom-call | tf_op jit(solution)/shard_map/pallas_call | solution.py:478
